TPU v7x, 32 devices: a whole 2x2x4 slice. The times are simulated.
32 devices in a mesh: fs: 16 (over z, y, x), tp: 2 (over core).
Axes of the slice: x: 2, y: 2, z: 4, core: 2. Of those that a mesh axis runs over, the one named last changes fastest.
Arguments:
- normed_input: bfloat16 [8192, 2048], P('fs', 'tp'), may hold values from -6 to 6
- cotangent: bfloat16 [8192, 2048], P('fs', 'tp'), may hold values from -6 to 6
- up_weight: bfloat16 [2048, 8192], P('fs', 'tp'), may hold values from -0.125 to 0.125
- down_weight: bfloat16 [8192, 2048], P('tp', 'fs'), may hold values from -0.0625 to 0.0625
Outputs:
- input_grad: bfloat16 [8192, 2048], P('fs', 'tp')
- up_grad: float32 [2048, 8192], P('fs', 'tp')
- down_grad: float32 [8192, 2048], P('tp', 'fs')
All inputs are finite; a program needn't handle non-finite values.
Results may differ from a plain program's by a relative error of at most 0.018.
Values may be sent and summed in bfloat16 or wider, within the bound.
No kernel may reach another device: no remote copies, remote signals or barrier semaphores. Data moves between devices by JAX's collectives and lax.ppermute only.
A program may use at most 192 MiB of HBM per device.

v0:
```python
import functools

import jax
import jax.numpy as jnp
from jax import lax
from jax.experimental import pallas as pl
from jax.experimental.pallas import tpu as pltpu
from jax.sharding import PartitionSpec as P


AXES = ("fs", "tp")
CHUNKS = 1
BF, F32 = jnp.bfloat16, jnp.float32


def dot(left, right, dims):
    return lax.dot_general(left, right, (dims, ((), ())), preferred_element_type=F32)


def place(buffer, piece, axis, index):
    return lax.dynamic_update_slice_in_dim(buffer, jnp.expand_dims(piece, axis), index, axis)


def pick(array, axis, index):
    return lax.dynamic_index_in_dim(array, index, axis, keepdims=False)


def plain(x, dy, up, down):
    n, m = lax.axis_size("fs"), lax.axis_size("tp")
    f, t = lax.axis_index("fs"), lax.axis_index("tp")
    rows, part = x.shape
    d_rows, ff = up.shape
    planes = n // 4
    px, py, pz = f % 2, (f // 2) % 2, f // 4
    scale = lax.rsqrt(jnp.asarray(rows * n, F32))
    turn = t * (planes // m) if planes >= m else 0

    def send(value, mask, core=0):
        perm = [(i * m + c, (i ^ mask) * m + (c ^ core)) for i in range(n) for c in range(m)]
        return lax.ppermute(value, AXES, perm)

    def tokens(value):
        near = send(value, 4)
        pieces = [value, send(value, 2), near, send(near, 2)]
        return jnp.concatenate(
            [jnp.concatenate([p] + [send(p, 0, c) for c in range(1, m)], axis=1) for p in pieces]
        )

    block = ff // 4
    width = block // CHUNKS

    def at(z):
        return z ^ turn

    def weights(w, chunk, rowwise):
        if rowwise:
            w = w.reshape(d_rows, 2, 2, CHUNKS, width)[:, :, :, chunk]
        else:
            w = w.reshape(2, 2, CHUNKS, width, d_rows)[:, :, chunk]
        ax = 1 if rowwise else 0
        mine, theirs = pick(w, ax, py), send(pick(w, ax, 1 - py), 2)
        both = place(place(jnp.zeros((2,) + mine.shape, BF), mine, 0, py), theirs, 0, 1 - py)
        zl = pz % 2
        got = {}
        halves = {b: pick(both, ax + 1, zl ^ b) for b in (0, 1)}
        for mask in range(planes):
            piece = halves[mask % 2]
            got[mask] = send(piece, 4 * mask) if mask else piece
        whole = jnp.zeros((planes,) + halves[0].shape, BF)
        for mask in range(planes):
            whole = place(whole, got[mask], 0, at(pz ^ mask))
        other = send(whole, 1)
        full = jnp.zeros((planes, 2, 2) + whole.shape[2:], BF)
        full = place(place(full, whole, 2, px), other, 2, 1 - px)
        if rowwise:
            return full.reshape(n * d_rows, width)
        return full.transpose(3, 0, 1, 2, 4).reshape(width, n * d_rows)

    def reduce_out(g, rowwise):
        g = (g * scale).astype(BF)
        if rowwise:
            g = g.reshape(planes, 2, 2, d_rows, width)
        else:
            g = g.reshape(width, planes, 2, 2, d_rows).transpose(1, 2, 3, 0, 4)
        mine, theirs = pick(g, 2, px), pick(g, 2, 1 - px)
        h = (mine.astype(F32) + send(theirs, 1).astype(F32)).astype(BF)
        total = [pick(h, 0, at(pz)).astype(F32), None]
        for mask in range(1, planes):
            got = send(pick(h, 0, at(pz ^ mask)), 4 * mask).astype(F32)
            b = mask % 2
            total[b] = got if total[b] is None else total[b] + got
        out = jnp.stack(total)
        mine, theirs = pick(out, 1, py), pick(out, 1, 1 - py)
        other = send(theirs.astype(BF), 2).astype(F32)
        return mine, other

    x4, dy4 = tokens(x), tokens(dy)
    zl = pz % 2
    dx = None
    ups, downs = [], []
    for chunk in range(CHUNKS):
        wu = weights(up, chunk, True)
        wd = weights(down, chunk, False)
        rect = jax.nn.relu(dot(x4, wu, ((1,), (0,))))
        act = (rect * rect).astype(BF)
        pre_grad = (2.0 * rect * dot(dy4, wd, ((1,), (1,)))).astype(BF)
        downs.append(reduce_out(dot(act, dy4, ((0,), (0,))), False))
        ups.append(reduce_out(dot(x4, pre_grad, ((0,), (0,))), True))
        term = dot(pre_grad, wu, ((1,), (1,)))
        dx = term if dx is None else dx + term

    dx = dx.astype(BF).reshape(4, rows, m, part)
    own = dx[:, :, 0].astype(F32)
    for c in range(1, m):
        own = own + send(dx[:, :, c], 0, c).astype(F32)
    near = own[0::2] + send(own[1::2].astype(BF), 2).astype(F32)
    input_grad = (near[0] + send(near[1].astype(BF), 4).astype(F32)).astype(BF)

    def join(parts, rowwise):
        out = jnp.zeros((2, 2, CHUNKS) + parts[0][0].shape[1:], F32)
        for chunk, (mine, other) in enumerate(parts):
            for value, y in ((mine, py), (other, 1 - py)):
                for b in (0, 1):
                    start = (y, zl ^ b, chunk) + (0,) * (out.ndim - 3)
                    out = lax.dynamic_update_slice(out, value[b][None, None, None], start)
        if rowwise:
            return out.transpose(3, 0, 1, 2, 4).reshape(d_rows, ff)
        return out.reshape(ff, d_rows)

    return input_grad, join(ups, True), join(downs, False)


LANES = 128
NT, NN, TN = ((1,), (1,)), ((1,), (0,)), ((0,), (0,))


def call(body, outs, scratch, sems, flops, args):
    nbytes = sum(a.size * a.dtype.itemsize for a in args) + sum(
        2 * functools.reduce(lambda p, q: p * q, o) for o in outs
    )
    return pl.pallas_call(
        body,
        out_shape=[jax.ShapeDtypeStruct(o, BF) for o in outs],
        in_specs=[pl.BlockSpec(memory_space=pltpu.SMEM)]
        + [pl.BlockSpec(memory_space=pl.ANY)] * (len(args) - 1),
        out_specs=[pl.BlockSpec(memory_space=pl.ANY)] * len(outs),
        scratch_shapes=[pltpu.VMEM(s, BF) for s in scratch]
        + [pltpu.SemaphoreType.DMA(s if isinstance(s, tuple) else (s,)) for s in sems],
        cost_estimate=pl.CostEstimate(flops=flops, bytes_accessed=nbytes, transcendentals=0),
        compiler_params=pltpu.CompilerParams(vmem_limit_bytes=26 * 2**20),
    )(*args)


def start(copies):
    for copy in copies:
        copy.start()
    return copies


def wait(copies):
    for copy in copies:
        copy.wait()


def weight_copies(base, pieces, dest, sem):
    copies = []
    for mz, row in enumerate(pieces):
        for kx, piece in enumerate(row):
            for ky in range(2):
                pos = pl.multiple_of((base ^ (mz * 4 + ky * 2 + kx)) * LANES, LANES)
                copies.append(
                    pltpu.make_async_copy(
                        piece.at[ky], dest.at[:, pl.ds(pos, LANES)], sem.at[len(copies)]
                    )
                )
    return copies


def token_copies(pieces, dest, sem):
    m = len(pieces[0])
    rows, part = pieces[0][0].shape
    return [
        [
            pltpu.make_async_copy(
                piece,
                dest.at[pl.ds(p * rows, rows), pl.ds(c * part, part)],
                sem.at[p * m + c],
            )
            for c, piece in enumerate(row)
        ]
        for p, row in enumerate(pieces)
    ]


def group(refs, count, size):
    return [refs[i * size : (i + 1) * size] for i in range(count)]


def hidden_kernel(planes, m, second, base_ref, *refs):
    tokens, refs = group(refs, 4, m), refs[4 * m :]
    weights, refs = group(refs, planes, 2), refs[2 * planes :]
    if second:
        rect, out, wv, tv, rv, ov, wsem, tsem, rsem, osem = refs
        outs = [(out, ov)]
    else:
        act, rect, wv, tv, rv, ov, wsem, tsem, osem = refs
        outs = [(act, ov), (rect, rv)]
    rows = tokens[0][0].shape[0]
    width = wv.shape[0]
    wcopies = start(weight_copies(base_ref[0], weights, wv, wsem))
    tcopies = token_copies(tokens, tv, tsem)
    for row in tcopies:
        start(row)
    if second:
        rcopies = start([pltpu.make_async_copy(rect.at[p], rv.at[p], rsem.at[p]) for p in range(4)])
    wait(wcopies)
    tile = min(width, 256)
    ocopies = []
    for p in range(4):
        wait(tcopies[p])
        if second:
            rcopies[p].wait()

        @pl.loop(0, width // tile)
        def _(i):
            at = pl.ds(pl.multiple_of(i * tile, tile), tile)
            o = dot(wv[at, :], tv[pl.ds(p * rows, rows), :], NT)
            if second:
                ov[p, at, :] = (2.0 * rv[p, at, :].astype(F32) * o).astype(BF)
            else:
                r = jnp.maximum(o, 0.0)
                rv[p, at, :] = r.astype(BF)
                ov[p, at, :] = (r * r).astype(BF)

        for k, (dest, source) in enumerate(outs):
            ocopies += start(
                [pltpu.make_async_copy(source.at[p], dest.at[p], osem.at[p * len(outs) + k])]
            )
    wait(ocopies)


def grad_kernel(planes, m, scale, base_ref, *refs):
    tokens, refs = group(refs, 4, m), refs[4 * m :]
    hidden, *outs, av, tv, ov, tsem, asem, osem = refs
    rows = tokens[0][0].shape[0]
    width = av.shape[0]
    base = base_ref[0]
    acopies = start(
        [
            pltpu.make_async_copy(hidden.at[p], av.at[:, pl.ds(p * rows, rows)], asem.at[p])
            for p in range(4)
        ]
    )
    tcopies = token_copies(tokens, tv, tsem)
    for c in range(m):
        start([row[c] for row in tcopies])
    wait(acopies)
    tile = min(width, 512)
    even = (base & 1) == 0
    each = 2 * planes // m

    def out_copies(mz, ky):
        return [
            pltpu.make_async_copy(
                ov.at[mz, k, ky], outs[2 * mz + k].at[ky], osem.at[mz, k, ky]
            )
            for k in range(2)
        ]

    for c in range(m):
        wait([row[c] for row in tcopies])

        @pl.loop(c * each, (c + 1) * each)
        def _(q):
            mask = (base >> 1) ^ q
            mz, ky = mask >> 1, mask & 1
            cols = pl.ds(pl.multiple_of(q * 2 * LANES, 2 * LANES), 2 * LANES)

            @pl.loop(0, width // tile)
            def _(i):
                at = pl.ds(pl.multiple_of(i * tile, tile), tile)
                o = dot(av[at, :], tv[:, cols], NN) * scale
                lo, hi = o[:, :LANES], o[:, LANES:]
                ov[mz, 0, ky, at, :] = jnp.where(even, lo, hi).astype(BF)
                ov[mz, 1, ky, at, :] = jnp.where(even, hi, lo).astype(BF)

            for plane in range(planes):

                @pl.when(mz == plane)
                def _():
                    start(out_copies(plane, ky))

    for plane in range(planes):
        for ky in range(2):
            wait(out_copies(plane, ky))


def input_kernel(planes, m, base_ref, *refs):
    hidden, refs = refs[0], refs[1:]
    weights, refs = group(refs, planes, 2), refs[2 * planes :]
    outs, (wv, av, ov, wsem, asem, osem) = refs[: 4 * m], refs[4 * m :]
    part = outs[0].shape[1]
    wcopies = start(weight_copies(base_ref[0], weights, wv, wsem))
    acopies = start([pltpu.make_async_copy(hidden.at[p], av.at[p], asem.at[p]) for p in range(4)])
    wait(wcopies)
    wait(acopies)
    ocopies = []
    for c in range(m - 1, -1, -1):
        for p in range(3, -1, -1):
            ov[c, p] = dot(av[p], wv[:, c * part : (c + 1) * part], TN).astype(BF)
            k = c * 4 + p
            ocopies += start([pltpu.make_async_copy(ov.at[c, p], outs[k], osem.at[k])])
    wait(ocopies)


def per_device(x, dy, up, down):
    n, m = lax.axis_size("fs"), lax.axis_size("tp")
    rows, part = x.shape
    d_rows, ff = up.shape
    planes = n // 4
    if d_rows != LANES or planes < m:
        return plain(x, dy, up, down)
    f, t = lax.axis_index("fs"), lax.axis_index("tp")
    py, zl = (f // 2) % 2, (f // 4) % 2
    base = (f ^ (4 * t * (planes // m))).astype(jnp.int32).reshape(1)
    width = ff // 4
    scale = float(rows * n) ** -0.5
    flops = 2 * 4 * rows * width * n * d_rows

    def send(value, mask, core=0):
        perm = [(i * m + c, (i ^ mask) * m + (c ^ core)) for i in range(n) for c in range(m)]
        return lax.ppermute(value, AXES, perm)

    def gather_tokens(value):
        near = send(value, 4)
        side = send(value, 2)
        pieces = (value, side, near, send(near, 2))
        return [[p] + [send(p, 0, c) for c in range(1, m)] for p in pieces]

    def gather_weights(w):
        w = w.reshape(2, 2, width, d_rows)
        mine, theirs = pick(w, 0, py), send(pick(w, 0, 1 - py), 2)
        both = jnp.stack([mine, theirs])
        halves = [pick(both, 1, zl), pick(both, 1, 1 - zl)]
        pieces = []
        for mz in range(planes):
            piece = send(halves[mz % 2], 4 * mz) if mz else halves[0]
            pieces.append([piece, send(piece, 1)])
        return pieces

    def flat(lists):
        return [a for row in lists for a in row]

    x4 = gather_tokens(x)
    wu = gather_weights(up.T)
    dy4 = gather_tokens(dy)
    wd = gather_weights(down)
    every = 4 * rows
    hid, feats = (4, width, rows), n * d_rows
    nw, nt = 4 * planes, 4 * m

    act, rect = call(
        functools.partial(hidden_kernel, planes, m, False),
        [hid, hid],
        [(width, feats), (every, feats), hid, hid],
        [nw, nt, 8],
        flops,
        [base, *flat(x4), *flat(wu)],
    )

    def grad(tokens, hidden):
        return call(
            functools.partial(grad_kernel, planes, m, scale),
            [(2, width, LANES)] * (2 * planes),
            [(width, every), (every, feats), (planes, 2, 2, width, LANES)],
            [nt, 4, (planes, 2, 2)],
            flops,
            [base, *flat(tokens), hidden],
        )

    def scatter(parts):
        total = [None, None]
        for mz in reversed(range(planes)):
            got = send(parts[2 * mz + 1], 1).astype(F32)
            value = parts[2 * mz].astype(F32) + got
            if mz:
                value = value.astype(BF)
            if mz:
                value = send(value, 4 * mz).astype(F32)
            b = mz % 2
            total[b] = value if total[b] is None else total[b] + value
        other = send(jnp.stack([total[0][1], total[1][1]]).astype(BF), 2)
        a, b = total[0][0], total[1][0]
        c, d = other[0].astype(F32), other[1].astype(F32)
        a, b = jnp.where(zl == 0, a, b), jnp.where(zl == 0, b, a)
        c, d = jnp.where(zl == 0, c, d), jnp.where(zl == 0, d, c)
        a, b, c, d = (
            jnp.where(py == 0, a, c),
            jnp.where(py == 0, b, d),
            jnp.where(py == 0, c, a),
            jnp.where(py == 0, d, b),
        )
        return jnp.concatenate([a, b, c, d])

    down_grad = scatter(grad(dy4, act))
    (pre_grad,) = call(
        functools.partial(hidden_kernel, planes, m, True),
        [hid],
        [(width, feats), (every, feats), hid, hid],
        [nw, nt, 4, 4],
        flops,
        [base, *flat(dy4), *flat(wd), rect],
    )
    up_grad = scatter(grad(x4, pre_grad)).T
    dx = call(
        functools.partial(input_kernel, planes, m),
        [(rows, part)] * (4 * m),
        [(width, feats), hid, (m, 4, rows, part)],
        [nw, 4, 4 * m],
        flops,
        [base, pre_grad, *flat(wu)],
    )
    own = [None] * 4
    for p in range(3, -1, -1):
        own[p] = dx[p].astype(F32)
        for c in range(1, m):
            own[p] = own[p] + send(dx[4 * c + p], 0, c).astype(F32)
    far = own[2] + send(own[3].astype(BF), 2).astype(F32)
    near = own[0] + send(own[1].astype(BF), 2).astype(F32)
    input_grad = (near + send(far.astype(BF), 4).astype(F32)).astype(BF)
    return input_grad, up_grad, down_grad


def solution(mesh):
    in_specs = (P("fs", "tp"), P("fs", "tp"), P("fs", "tp"), P("tp", "fs"))
    out_specs = (P("fs", "tp"), P("fs", "tp"), P("tp", "fs"))

    return jax.shard_map(
        per_device, mesh=mesh, in_specs=in_specs, out_specs=out_specs, check_vma=False
    )
```

profile of v0, /device:TPU:0, one launch (start us, length us, event | category | flops | bytes accessed | tf_op | source)
XLA Modules:
  0.0 478.6 jit_solution(12625197771667092753)
XLA Ops:
  0.7 1.8 reshape.53
  4.4 3.0 collective-permute-start.22
  9.0 11.4 %collective-permute-done.22 = bf16[2,1024,128]{2,1,0:T(8,128)(2,1)S(1)} collective-permute-done((bf16[2,1024,128]{2,1,0:T(8,128)(2,1)}, bf16[2,1024,128]{2,1,0:T(8,128)(2,1)S(1)}, u32[]{:S(2)}, u32[]{:S(2)}) %collective-permute-start.22) | collective-permute-done | bytes 524320 | tf_op jit(solution)/shard_map/ppermute | solution.py:332
  20.5 2.1 collective-permute-start.24
  22.7 3.0 collective-permute-start.26
  27.1 3.9 collective-permute-done.7
  30.9 1.7 collective-permute-start.16
  32.7 13.9 %collective-permute-done.24.refs_10_.refs_3_ = bf16[2,1024,128]{2,1,0:T(8,128)(2,1)S(1)} collective-permute-done((bf16[2,1024,128]{2,1,0:T(8,128)(2,1)S(1)}, bf16[2,1024,128]{2,1,0:T(8,128)(2,1)S(1)}, u32[]{:S(2)}, u32[]{:S(2)}) %collective-permute-start.24) | collective-permute-done | bytes 524320 | tf_op jit(solution)/shard_map/ppermute | solution.py:332
  46.5 1.4 collective-permute-start.23
  48.0 20.7 %collective-permute-done.26.refs_12_.refs_5_ = bf16[2,1024,128]{2,1,0:T(8,128)(2,1)S(1)} collective-permute-done((bf16[2,1024,128]{2,1,0:T(8,128)(2,1)S(1)}, bf16[2,1024,128]{2,1,0:T(8,128)(2,1)S(1)}, u32[]{:S(2)}, u32[]{:S(2)}) %collective-permute-start.26) | collective-permute-done | bytes 524320 | tf_op jit(solution)/shard_map/ppermute | solution.py:332
  68.7 11.8 %collective-permute-done.28.refs_14_.refs_7_ = bf16[2,1024,128]{2,1,0:T(8,128)(2,1)S(1)} collective-permute-done((bf16[2,1024,128]{2,1,0:T(8,128)(2,1)S(1)}, bf16[2,1024,128]{2,1,0:T(8,128)(2,1)S(1)}, u32[]{:S(2)}, u32[]{:S(2)}) %collective-permute-start.28) | collective-permute-done | bytes 524320 | tf_op jit(solution)/shard_map/ppermute | solution.py:332
  81.4 1.5 collective-permute-start.1
  85.6 2.0 collective-permute-start.9
  87.6 19.1 %collective-permute-done.3.refs_4_ = bf16[512,1024]{1,0:T(8,128)(2,1)} collective-permute-done((bf16[512,1024]{1,0:T(8,128)(2,1)S(1)}, bf16[512,1024]{1,0:T(8,128)(2,1)}, u32[]{:S(2)}, u32[]{:S(2)}) %collective-permute-start.3) | collective-permute-done | bytes 1048608 | tf_op jit(solution)/shard_map/ppermute | solution.py:332
  106.7 1.5 collective-permute-start.25
  110.0 3.6 collective-permute-done.9.refs_10_
  113.6 1.5 collective-permute-start.5
  115.2 2.7 collective-permute-done.25.refs_11_.refs_4_
  118.7 11.3 %collective-permute-done.20.refs_6_ = bf16[512,1024]{1,0:T(8,128)(2,1)} collective-permute-done((bf16[512,1024]{1,0:T(8,128)(2,1)S(1)}, bf16[512,1024]{1,0:T(8,128)(2,1)}, u32[]{:S(2)}, u32[]{:S(2)}) %collective-permute-start.20) | collective-permute-done | bytes 1048608 | tf_op jit(solution)/shard_map/ppermute | solution.py:332
  130.8 1.5 collective-permute-start.29
  132.3 12.8 %collective-permute-done.29.refs_15_.refs_8_ = bf16[2,1024,128]{2,1,0:T(8,128)(2,1)S(1)} collective-permute-done((bf16[2,1024,128]{2,1,0:T(8,128)(2,1)S(1)}, bf16[2,1024,128]{2,1,0:T(8,128)(2,1)S(1)}, u32[]{:S(2)}, u32[]{:S(2)}) %collective-permute-start.29) | collective-permute-done | bytes 524320 | tf_op jit(solution)/shard_map/ppermute | solution.py:332
  147.7 1.4 collective-permute-start.13
  149.1 2.0 collective-permute-start.11
  160.0 15.2 %shard_map.67 = (bf16[4,1024,512]{2,1,0:T(8,128)(2,1)S(1)}, bf16[4,1024,512]{2,1,0:T(8,128)(2,1)S(1)}) custom-call(s32[1]{0:T(128)} %bitcast.base_ref, bf16[512,1024]{1,0:T(8,128)(2,1)} %refs_0_.6, bf16[512,1024]{1,0:T(8,128)(2,1)S(1)} %copy-done.4, bf16[512,1024]{1,0:T(8,128)(2,1)} %collective-permute-done.16.refs_2_, ...), custom_call_target="tpu_custom_call" | custom-call | flops 8589934592 | bytes 20971524 | tf_op jit(solution)/shard_map/pallas_call | solution.py:141
  175.2 22.0 %collective-permute-done.11.refs_12_ = bf16[2,1024,128]{2,1,0:T(8,128)(2,1)S(1)} collective-permute-done((bf16[2,1024,128]{2,1,0:T(8,128)(2,1)S(1)}, bf16[2,1024,128]{2,1,0:T(8,128)(2,1)S(1)}, u32[]{:S(2)}, u32[]{:S(2)}) %collective-permute-start.11) | collective-permute-done | bytes 524320 | tf_op jit(solution)/shard_map/ppermute | solution.py:332
  197.2 1.5 collective-permute-start.8
  199.2 1.5 collective-permute-start.12
  201.3 15.3 %shard_map.71 = (bf16[2,1024,128]{2,1,0:T(8,128)(2,1)S(1)}, bf16[2,1024,128]{2,1,0:T(8,128)(2,1)S(1)}, bf16[2,1024,128]{2,1,0:T(8,128)(2,1)S(1)}, bf16[2,1024,12...) custom-call(s32[1]{0:T(128)} %bitcast.base_ref, ...), custom_call_target="tpu_custom_call" | custom-call | flops 8589934592 | bytes 16777220 | tf_op jit(solution)/shard_map/pallas_call | solution.py:141
  216.6 1.5 collective-permute-start.45
  218.7 4.5 collective-permute-done.10.refs_11_
  223.2 1.5 collective-permute-start.48
  224.7 9.7 %collective-permute-done.12.refs_13_ = bf16[2,1024,128]{2,1,0:T(8,128)(2,1)S(1)} collective-permute-done((bf16[2,1024,128]{2,1,0:T(8,128)(2,1)S(1)}, bf16[2,1024,128]{2,1,0:T(8,128)(2,1)S(1)}, u32[]{:S(2)}, u32[]{:S(2)}) %collective-permute-start.12) | collective-permute-done | bytes 524320 | tf_op jit(solution)/shard_map/ppermute | solution.py:332
  234.5 1.5 collective-permute-start.50
  236.0 9.7 %collective-permute-done.14.refs_15_ = bf16[2,1024,128]{2,1,0:T(8,128)(2,1)S(1)} collective-permute-done((bf16[2,1024,128]{2,1,0:T(8,128)(2,1)S(1)}, bf16[2,1024,128]{2,1,0:T(8,128)(2,1)S(1)}, u32[]{:S(2)}, u32[]{:S(2)}) %collective-permute-start.14) | collective-permute-done | bytes 524320 | tf_op jit(solution)/shard_map/ppermute | solution.py:332
  245.7 14.6 %shard_map.68.refs_0_.refs_8_ = bf16[4,1024,512]{2,1,0:T(8,128)(2,1)S(1)} custom-call(s32[1]{0:T(128)} %bitcast.base_ref, bf16[512,1024]{1,0:T(8,128)(2,1)S(1)} %copy-done, bf16[512,1024]{1,0:T(8,128)(2,1)S(1)} %copy-done.7, bf16[512,1024]{1,0:T(8,128)(2,1)} %collective-permute-done.1.refs_2_, bf16[512,1024]{1,0:T(8,128)(2,1)} %collective-permute-done.2.refs_3_, ...), custom_call_target="tpu_custom_call" | custom-call | flops 8589934592 | bytes 20971524 | tf_op jit(solution)/shard_map/pallas_call | solution.py:141
  260.3 2.0 copy-done.29
  262.3 2.2 copy-done.30
  264.6 15.4 %shard_map.70 = (bf16[2,1024,128]{2,1,0:T(8,128)(2,1)S(1)}, bf16[2,1024,128]{2,1,0:T(8,128)(2,1)S(1)}, bf16[2,1024,128]{2,1,0:T(8,128)(2,1)S(1)}, bf16[2,1024,12...) custom-call(s32[1]{0:T(128)} %bitcast.base_ref, ...), custom_call_target="tpu_custom_call" | custom-call | flops 8589934592 | bytes 16777220 | tf_op jit(solution)/shard_map/pallas_call | solution.py:141
  279.9 1.6 collective-permute-start.37
  281.5 2.2 copy-done.31
  283.7 12.8 %shard_map.69 = (bf16[512,1024]{1,0:T(8,128)(2,1)S(1)}, bf16[512,1024]{1,0:T(8,128)(2,1)S(1)}, bf16[512,1024]{1,0:T(8,128)(2,1)S(1)}, bf16[512,1024]{1,0:T(8,128...) custom-call(s32[1]{0:T(128)} %bitcast.base_ref, ...), custom_call_target="tpu_custom_call" | custom-call | flops 8589934592 | bytes 16777220 | tf_op jit(solution)/shard_map/pallas_call | solution.py:141
  297.3 1.6 collective-permute-start.40
  299.8 2.1 collective-permute-done.37
  302.0 22.3 %collective-permute-done.40 = bf16[2,1024,128]{2,1,0:T(8,128)(2,1)S(1)} collective-permute-done((bf16[2,1024,128]{2,1,0:T(8,128)(2,1)S(1)}, bf16[2,1024,128]{2,1,0:T(8,128)(2,1)S(1)}, u32[]{:S(2)}, u32[]{:S(2)}) %collective-permute-start.40) | collective-permute-done | bytes 524320 | tf_op jit(solution)/shard_map/ppermute | solution.py:332
  324.5 9.7 %collective-permute-done.42 = bf16[2,1024,128]{2,1,0:T(8,128)(2,1)S(1)} collective-permute-done((bf16[2,1024,128]{2,1,0:T(8,128)(2,1)S(1)}, bf16[2,1024,128]{2,1,0:T(8,128)(2,1)S(1)}, u32[]{:S(2)}, u32[]{:S(2)}) %collective-permute-start.42) | collective-permute-done | bytes 524320 | tf_op jit(solution)/shard_map/ppermute | solution.py:332
  335.6 33.2 %collective-permute-done.46 = bf16[2,1024,128]{2,1,0:T(8,128)(2,1)S(1)} collective-permute-done((bf16[2,1024,128]{2,1,0:T(8,128)(2,1)S(1)}, bf16[2,1024,128]{2,1,0:T(8,128)(2,1)S(1)}, u32[]{:S(2)}, u32[]{:S(2)}) %collective-permute-start.46) | collective-permute-done | bytes 524320 | tf_op jit(solution)/shard_map/ppermute | solution.py:332
  369.1 11.0 %collective-permute-done.38 = bf16[2,1024,128]{2,1,0:T(8,128)(2,1)S(1)} collective-permute-done((bf16[2,1024,128]{2,1,0:T(8,128)(2,1)S(1)}, bf16[2,1024,128]{2,1,0:T(8,128)(2,1)S(1)}, u32[]{:S(2)}, u32[]{:S(2)}) %collective-permute-start.38) | collective-permute-done | bytes 524320 | tf_op jit(solution)/shard_map/ppermute | solution.py:332
  380.3 2.6 collective-permute-start.49
  382.9 19.5 %collective-permute-done.43 = bf16[2,1024,128]{2,1,0:T(8,128)(2,1)S(1)} collective-permute-done((bf16[2,1024,128]{2,1,0:T(8,128)(2,1)S(1)}, bf16[2,1024,128]{2,1,0:T(8,128)(2,1)S(1)}, u32[]{:S(2)}, u32[]{:S(2)}) %collective-permute-start.43) | collective-permute-done | bytes 524320 | tf_op jit(solution)/shard_map/ppermute | solution.py:332
  402.4 2.3 collective-permute-start.51
  405.3 1.6 collective-permute-start.35
  407.0 9.5 %collective-permute-done.51 = bf16[2,1024,128]{2,1,0:T(8,128)(2,1)S(1)} collective-permute-done((bf16[2,1024,128]{2,1,0:T(8,128)(2,1)S(1)}, bf16[2,1024,128]{2,1,0:T(8,128)(2,1)S(1)}, u32[]{:S(2)}, u32[]{:S(2)}) %collective-permute-start.51) | collective-permute-done | bytes 524320 | tf_op jit(solution)/shard_map/ppermute | solution.py:332
  416.5 1.5 collective-permute-start.44
  419.8 1.4 add_convert_fusion.3
  421.2 21.4 %collective-permute-done.44 = bf16[2,1024,128]{2,1,0:T(8,128)(2,1)S(1)} collective-permute-done((bf16[2,1024,128]{2,1,0:T(8,128)(2,1)S(1)}, bf16[2,1024,128]{2,1,0:T(8,128)(2,1)S(1)}, u32[]{:S(2)}, u32[]{:S(2)}) %collective-permute-start.44) | collective-permute-done | bytes 524320 | tf_op jit(solution)/shard_map/ppermute | solution.py:332
  442.6 1.5 collective-permute-start.32
  444.3 1.6 add_convert_fusion.1
  445.9 1.5 maximum_bitcast_fusion
  447.4 2.9 copy.10
  450.2 3.7 collective-permute-done.52
  453.9 1.4 select_bitcast_fusion.3
  455.3 1.5 pad_maximum_fusion
  456.8 18.1 %collective-permute-done.32 = bf16[512,1024]{1,0:T(8,128)(2,1)} collective-permute-done((bf16[512,1024]{1,0:T(8,128)(2,1)}, bf16[512,1024]{1,0:T(8,128)(2,1)}, u32[]{:S(2)}, u32[]{:S(2)}) %collective-permute-start.32) | collective-permute-done | bytes 1048608 | tf_op jit(solution)/shard_map/ppermute | solution.py:332
  474.9 3.7 add_convert_fusion
  (151 shorter events, 31.5 us)
Async XLA Ops:
  4.4 16.0 %collective-permute-start.22 = (bf16[2,1024,128]{2,1,0:T(8,128)(2,1)}, bf16[2,1024,128]{2,1,0:T(8,128)(2,1)S(1)}, u32[]{:S(2)}, u32[]{:S(2)}) collective-permute-start(bf16[2,1024,128]{2,1,0:T(8,128)(2,1)} %bitcast.7), channel_id=1, source_target_pairs={{0,4},{1,5},{2,6},{3,7},{4,0},{5,1},{6,2},{7,3},{8,12},{9,13},{10,... | collective-permute-start | bytes 1572872 | tf_op jit(solution)/shard_map/ppermute | solution.py:332
  8.5 72.1 %copy-start = (bf16[512,1024]{1,0:T(8,128)(2,1)S(1)}, bf16[512,1024]{1,0:T(8,128)(2,1)}, u32[]{:S(2)}) copy-start(bf16[512,1024]{1,0:T(8,128)(2,1)} %refs_0_.7) | copy-start | bytes 3145732
  8.5 22.4 %collective-permute-start.7 = (bf16[2,1024,128]{2,1,0:T(8,128)(2,1)}, bf16[2,1024,128]{2,1,0:T(8,128)(2,1)}, u32[]{:S(2)}, u32[]{:S(2)}) collective-permute-start(bf16[2,1024,128]{2,1,0:T(8,128)(2,1)} %get-tuple-element.72), channel_id=1, source_target_pairs={{0,4},{1,5},{2,6},{3,7},{4,0},{5,1},{6,2},{7,3},{8,12},{9,13},{10,... | collective-permute-start | bytes 1572872 | tf_op jit(solution)/shard_map/ppermute | solution.py:332
  9.0 74.5 %copy-start.33 = (bf16[1,2,1024,128]{3,2,0,1:T(8,128)(2,1)S(1)}, bf16[1,2,1024,128]{3,2,0,1:T(8,128)(2,1)}, u32[]{:S(2)}) copy-start(bf16[1,2,1024,128]{3,2,0,1:T(8,128)(2,1)} %get-tuple-element.73) | copy-start | bytes 1572868
  20.5 26.0 %collective-permute-start.24 = (bf16[2,1024,128]{2,1,0:T(8,128)(2,1)S(1)}, bf16[2,1024,128]{2,1,0:T(8,128)(2,1)S(1)}, u32[]{:S(2)}, u32[]{:S(2)}) collective-permute-start(bf16[2,1024,128]{2,1,0:T(8,128)(2,1)S(1)} %get-tuple-element.66), channel_id=1, source_target_pairs={{0,8},{1,9},{2,10},{3,11},{4,12},{5,13},{6,14},{7,15},{8,0},{9,1},... | collective-permute-start | bytes 1572872 | tf_op jit(solution)/shard_map/ppermute | solution.py:332
  22.7 60.2 %collective-permute-start.18 = (bf16[512,1024]{1,0:T(8,128)(2,1)}, bf16[512,1024]{1,0:T(8,128)(2,1)S(1)}, u32[]{:S(2)}, u32[]{:S(2)}) collective-permute-start(bf16[512,1024]{1,0:T(8,128)(2,1)} %refs_0_.6), channel_id=1, source_target_pairs={{0,8},{1,9},{2,10},{3,11},{4,12},{5,13},{6,14},{7,15},{8,0},{9,1},... | collective-permute-start | bytes 3145736 | tf_op jit(solution)/shard_map/ppermute | solution.py:332
  22.7 45.9 %collective-permute-start.26 = (bf16[2,1024,128]{2,1,0:T(8,128)(2,1)S(1)}, bf16[2,1024,128]{2,1,0:T(8,128)(2,1)S(1)}, u32[]{:S(2)}, u32[]{:S(2)}) collective-permute-start(bf16[2,1024,128]{2,1,0:T(8,128)(2,1)S(1)} %get-tuple-element.67.refs_8_.refs_1_), channel_id=1, source_target_pairs={{0,16},{1,17},{2,18},{3,19},{4,20},{5,21},{6,22},{7,23},{8,24},{9,... | collective-permute-start | bytes 1572872 | tf_op jit(solution)/shard_map/ppermute | solution.py:332
  25.7 54.8 %collective-permute-start.28 = (bf16[2,1024,128]{2,1,0:T(8,128)(2,1)S(1)}, bf16[2,1024,128]{2,1,0:T(8,128)(2,1)S(1)}, u32[]{:S(2)}, u32[]{:S(2)}) collective-permute-start(bf16[2,1024,128]{2,1,0:T(8,128)(2,1)S(1)} %get-tuple-element.66), channel_id=1, source_target_pairs={{0,24},{1,25},{2,26},{3,27},{4,28},{5,29},{6,30},{7,31},{8,16},{9,... | collective-permute-start | bytes 1572872 | tf_op jit(solution)/shard_map/ppermute | solution.py:332
  30.9 52.0 %collective-permute-start.16 = (bf16[512,1024]{1,0:T(8,128)(2,1)}, bf16[512,1024]{1,0:T(8,128)(2,1)}, u32[]{:S(2)}, u32[]{:S(2)}) collective-permute-start(bf16[512,1024]{1,0:T(8,128)(2,1)} %refs_0_.6), channel_id=1, source_target_pairs={{0,4},{1,5},{2,6},{3,7},{4,0},{5,1},{6,2},{7,3},{8,12},{9,13},{10,... | collective-permute-start | bytes 3145736 | tf_op jit(solution)/shard_map/ppermute | solution.py:332
  46.5 34.0 %collective-permute-start.23 = (bf16[2,1024,128]{2,1,0:T(8,128)(2,1)S(1)}, bf16[2,1024,128]{2,1,0:T(8,128)(2,1)S(1)}, u32[]{:S(2)}, u32[]{:S(2)}) collective-permute-start(bf16[2,1024,128]{2,1,0:T(8,128)(2,1)S(1)} %get-tuple-element.67.refs_8_.refs_1_), channel_id=1, source_target_pairs={{0,2},{1,3},{2,0},{3,1},{4,6},{5,7},{6,4},{7,5},{8,10},{9,11},{10,... | collective-permute-start | bytes 1572872 | tf_op jit(solution)/shard_map/ppermute | solution.py:332
  68.7 106.5 %copy-start.10 = (bf16[2,1024,128]{2,1,0:T(8,128)(2,1)}, bf16[2,1024,128]{2,1,0:T(8,128)(2,1)S(1)}, u32[]{:S(2)}) copy-start(bf16[2,1024,128]{2,1,0:T(8,128)(2,1)S(1)} %collective-permute-done.26.refs_12_.refs_5_) | copy-start | bytes 1572868
  68.7 15.9 %collective-permute-start.15 = (bf16[512,1024]{1,0:T(8,128)(2,1)}, bf16[512,1024]{1,0:T(8,128)(2,1)S(1)}, u32[]{:S(2)}, u32[]{:S(2)}) collective-permute-start(bf16[512,1024]{1,0:T(8,128)(2,1)} %refs_0_.6), channel_id=1, source_target_pairs={{0,1},{1,0},{2,3},{3,2},{4,5},{5,4},{6,7},{7,6},{8,9},{9,8},{10,11... | collective-permute-start | bytes 3145736 | tf_op jit(solution)/shard_map/ppermute | solution.py:332
  80.5 65.4 %copy-start.12 = (bf16[2,1024,128]{2,1,0:T(8,128)(2,1)}, bf16[2,1024,128]{2,1,0:T(8,128)(2,1)S(1)}, u32[]{:S(2)}) copy-start(bf16[2,1024,128]{2,1,0:T(8,128)(2,1)S(1)} %collective-permute-done.28.refs_14_.refs_7_) | copy-start | bytes 1572868
  80.5 26.1 %collective-permute-start.3 = (bf16[512,1024]{1,0:T(8,128)(2,1)S(1)}, bf16[512,1024]{1,0:T(8,128)(2,1)}, u32[]{:S(2)}, u32[]{:S(2)}) collective-permute-start(bf16[512,1024]{1,0:T(8,128)(2,1)S(1)} %copy-done), channel_id=1, source_target_pairs={{0,8},{1,9},{2,10},{3,11},{4,12},{5,13},{6,14},{7,15},{8,0},{9,1},... | collective-permute-start | bytes 3145736 | tf_op jit(solution)/shard_map/ppermute | solution.py:332
  81.4 26.8 %collective-permute-start.1 = (bf16[512,1024]{1,0:T(8,128)(2,1)S(1)}, bf16[512,1024]{1,0:T(8,128)(2,1)}, u32[]{:S(2)}, u32[]{:S(2)}) collective-permute-start(bf16[512,1024]{1,0:T(8,128)(2,1)S(1)} %copy-done), channel_id=1, source_target_pairs={{0,4},{1,5},{2,6},{3,7},{4,0},{5,1},{6,2},{7,3},{8,12},{9,13},{10,... | collective-permute-start | bytes 3145736 | tf_op jit(solution)/shard_map/ppermute | solution.py:332
  82.9 26.1 %copy-start.1 = (bf16[512,1024]{1,0:T(8,128)(2,1)}, bf16[512,1024]{1,0:T(8,128)(2,1)S(1)}, u32[]{:S(2)}) copy-start(bf16[512,1024]{1,0:T(8,128)(2,1)S(1)} %collective-permute-done.18.refs_4_) | copy-start | bytes 3145732
  82.9 26.1 %collective-permute-start = (bf16[512,1024]{1,0:T(8,128)(2,1)S(1)}, bf16[512,1024]{1,0:T(8,128)(2,1)S(1)}, u32[]{:S(2)}, u32[]{:S(2)}) collective-permute-start(bf16[512,1024]{1,0:T(8,128)(2,1)S(1)} %copy-done), channel_id=1, source_target_pairs={{0,1},{1,0},{2,3},{3,2},{4,5},{5,4},{6,7},{7,6},{8,9},{9,8},{10,11... | collective-permute-start | bytes 3145736 | tf_op jit(solution)/shard_map/ppermute | solution.py:332
  82.9 47.1 %collective-permute-start.20 = (bf16[512,1024]{1,0:T(8,128)(2,1)S(1)}, bf16[512,1024]{1,0:T(8,128)(2,1)}, u32[]{:S(2)}, u32[]{:S(2)}) collective-permute-start(bf16[512,1024]{1,0:T(8,128)(2,1)S(1)} %collective-permute-done.18.refs_4_), channel_id=1, source_target_pairs={{0,4},{1,5},{2,6},{3,7},{4,0},{5,1},{6,2},{7,3},{8,12},{9,13},{10,... | collective-permute-start | bytes 3145736 | tf_op jit(solution)/shard_map/ppermute | solution.py:332
  84.6 63.1 %copy-start.35 = (bf16[2,1024,128]{2,1,0:T(8,128)(2,1)}, bf16[2,1024,128]{2,1,0:T(8,128)(2,1)S(1)}, u32[]{:S(2)}) copy-start(bf16[2,1024,128]{2,1,0:T(8,128)(2,1)S(1)} %get-tuple-element.70) | copy-start | bytes 1572868
  85.6 28.0 %collective-permute-start.9 = (bf16[2,1024,128]{2,1,0:T(8,128)(2,1)S(1)}, bf16[2,1024,128]{2,1,0:T(8,128)(2,1)S(1)}, u32[]{:S(2)}, u32[]{:S(2)}) collective-permute-start(bf16[2,1024,128]{2,1,0:T(8,128)(2,1)S(1)} %get-tuple-element.70), channel_id=1, source_target_pairs={{0,8},{1,9},{2,10},{3,11},{4,12},{5,13},{6,14},{7,15},{8,0},{9,1},... | collective-permute-start | bytes 1572872 | tf_op jit(solution)/shard_map/ppermute | solution.py:332
  106.7 11.2 %collective-permute-start.25 = (bf16[2,1024,128]{2,1,0:T(8,128)(2,1)S(1)}, bf16[2,1024,128]{2,1,0:T(8,128)(2,1)S(1)}, u32[]{:S(2)}, u32[]{:S(2)}) collective-permute-start(bf16[2,1024,128]{2,1,0:T(8,128)(2,1)S(1)} %collective-permute-done.24.refs_10_.refs_3_), channel_id=1, source_target_pairs={{0,2},{1,3},{2,0},{3,1},{4,6},{5,7},{6,4},{7,5},{8,10},{9,11},{10,... | collective-permute-start | bytes 1572872 | tf_op jit(solution)/shard_map/ppermute | solution.py:332
  108.2 21.8 %collective-permute-start.27 = (bf16[2,1024,128]{2,1,0:T(8,128)(2,1)S(1)}, bf16[2,1024,128]{2,1,0:T(8,128)(2,1)S(1)}, u32[]{:S(2)}, u32[]{:S(2)}) collective-permute-start(bf16[2,1024,128]{2,1,0:T(8,128)(2,1)S(1)} %collective-permute-done.26.refs_12_.refs_5_), channel_id=1, source_target_pairs={{0,2},{1,3},{2,0},{3,1},{4,6},{5,7},{6,4},{7,5},{8,10},{9,11},{10,... | collective-permute-start | bytes 1572872 | tf_op jit(solution)/shard_map/ppermute | solution.py:332
  110.0 36.0 %collective-permute-start.19 = (bf16[512,1024]{1,0:T(8,128)(2,1)S(1)}, bf16[512,1024]{1,0:T(8,128)(2,1)S(1)}, u32[]{:S(2)}, u32[]{:S(2)}) collective-permute-start(bf16[512,1024]{1,0:T(8,128)(2,1)S(1)} %collective-permute-done.18.refs_4_), channel_id=1, source_target_pairs={{0,1},{1,0},{2,3},{3,2},{4,5},{5,4},{6,7},{7,6},{8,9},{9,8},{10,11... | collective-permute-start | bytes 3145736 | tf_op jit(solution)/shard_map/ppermute | solution.py:332
  113.6 33.8 %copy-start.24 = (bf16[2,1024,128]{2,1,0:T(8,128)(2,1)}, bf16[2,1024,128]{2,1,0:T(8,128)(2,1)S(1)}, u32[]{:S(2)}) copy-start(bf16[2,1024,128]{2,1,0:T(8,128)(2,1)S(1)} %collective-permute-done.9.refs_10_) | copy-start | bytes 1572868
  113.6 34.0 %collective-permute-start.5 = (bf16[512,1024]{1,0:T(8,128)(2,1)}, bf16[512,1024]{1,0:T(8,128)(2,1)}, u32[]{:S(2)}, u32[]{:S(2)}) collective-permute-start(bf16[512,1024]{1,0:T(8,128)(2,1)} %collective-permute-done.3.refs_4_), channel_id=1, source_target_pairs={{0,4},{1,5},{2,6},{3,7},{4,0},{5,1},{6,2},{7,3},{8,12},{9,13},{10,... | collective-permute-start | bytes 3145736 | tf_op jit(solution)/shard_map/ppermute | solution.py:332
  118.7 29.0 %collective-permute-start.17 = (bf16[512,1024]{1,0:T(8,128)(2,1)}, bf16[512,1024]{1,0:T(8,128)(2,1)}, u32[]{:S(2)}, u32[]{:S(2)}) collective-permute-start(bf16[512,1024]{1,0:T(8,128)(2,1)} %collective-permute-done.16.refs_2_), channel_id=1, source_target_pairs={{0,1},{1,0},{2,3},{3,2},{4,5},{5,4},{6,7},{7,6},{8,9},{9,8},{10,11... | collective-permute-start | bytes 3145736 | tf_op jit(solution)/shard_map/ppermute | solution.py:332
  130.0 19.1 %collective-permute-start.21 = (bf16[512,1024]{1,0:T(8,128)(2,1)}, bf16[512,1024]{1,0:T(8,128)(2,1)}, u32[]{:S(2)}, u32[]{:S(2)}) collective-permute-start(bf16[512,1024]{1,0:T(8,128)(2,1)} %collective-permute-done.20.refs_6_), channel_id=1, source_target_pairs={{0,1},{1,0},{2,3},{3,2},{4,5},{5,4},{6,7},{7,6},{8,9},{9,8},{10,11... | collective-permute-start | bytes 3145736 | tf_op jit(solution)/shard_map/ppermute | solution.py:332
  130.8 14.3 %collective-permute-start.29 = (bf16[2,1024,128]{2,1,0:T(8,128)(2,1)S(1)}, bf16[2,1024,128]{2,1,0:T(8,128)(2,1)S(1)}, u32[]{:S(2)}, u32[]{:S(2)}) collective-permute-start(bf16[2,1024,128]{2,1,0:T(8,128)(2,1)S(1)} %collective-permute-done.28.refs_14_.refs_7_), channel_id=1, source_target_pairs={{0,2},{1,3},{2,0},{3,1},{4,6},{5,7},{6,4},{7,5},{8,10},{9,11},{10,... | collective-permute-start | bytes 1572872 | tf_op jit(solution)/shard_map/ppermute | solution.py:332
  145.9 53.3 %collective-permute-start.4 = (bf16[512,1024]{1,0:T(8,128)(2,1)}, bf16[512,1024]{1,0:T(8,128)(2,1)}, u32[]{:S(2)}, u32[]{:S(2)}) collective-permute-start(bf16[512,1024]{1,0:T(8,128)(2,1)} %collective-permute-done.3.refs_4_), channel_id=1, source_target_pairs={{0,1},{1,0},{2,3},{3,2},{4,5},{5,4},{6,7},{7,6},{8,9},{9,8},{10,11... | collective-permute-start | bytes 3145736 | tf_op jit(solution)/shard_map/ppermute | solution.py:332
  146.9 53.8 %collective-permute-start.2 = (bf16[512,1024]{1,0:T(8,128)(2,1)}, bf16[512,1024]{1,0:T(8,128)(2,1)}, u32[]{:S(2)}, u32[]{:S(2)}) collective-permute-start(bf16[512,1024]{1,0:T(8,128)(2,1)} %collective-permute-done.1.refs_2_), channel_id=1, source_target_pairs={{0,1},{1,0},{2,3},{3,2},{4,5},{5,4},{6,7},{7,6},{8,9},{9,8},{10,11... | collective-permute-start | bytes 3145736 | tf_op jit(solution)/shard_map/ppermute | solution.py:332
  147.7 53.6 %collective-permute-start.6 = (bf16[512,1024]{1,0:T(8,128)(2,1)}, bf16[512,1024]{1,0:T(8,128)(2,1)}, u32[]{:S(2)}, u32[]{:S(2)}) collective-permute-start(bf16[512,1024]{1,0:T(8,128)(2,1)} %collective-permute-done.5.refs_6_), channel_id=1, source_target_pairs={{0,1},{1,0},{2,3},{3,2},{4,5},{5,4},{6,7},{7,6},{8,9},{9,8},{10,11... | collective-permute-start | bytes 3145736 | tf_op jit(solution)/shard_map/ppermute | solution.py:332
  147.7 51.0 %collective-permute-start.13 = (bf16[2,1024,128]{2,1,0:T(8,128)(2,1)}, bf16[2,1024,128]{2,1,0:T(8,128)(2,1)S(1)}, u32[]{:S(2)}, u32[]{:S(2)}) collective-permute-start(bf16[2,1024,128]{2,1,0:T(8,128)(2,1)} %copy-done.35), channel_id=1, source_target_pairs={{0,24},{1,25},{2,26},{3,27},{4,28},{5,29},{6,30},{7,31},{8,16},{9,... | collective-permute-start | bytes 1572872 | tf_op jit(solution)/shard_map/ppermute | solution.py:332
  149.1 48.1 %collective-permute-start.11 = (bf16[2,1024,128]{2,1,0:T(8,128)(2,1)S(1)}, bf16[2,1024,128]{2,1,0:T(8,128)(2,1)S(1)}, u32[]{:S(2)}, u32[]{:S(2)}) collective-permute-start(bf16[2,1024,128]{2,1,0:T(8,128)(2,1)S(1)} %get-tuple-element.71.refs_8_), channel_id=1, source_target_pairs={{0,16},{1,17},{2,18},{3,19},{4,20},{5,21},{6,22},{7,23},{8,24},{9,... | collective-permute-start | bytes 1572872 | tf_op jit(solution)/shard_map/ppermute | solution.py:332
  160.0 38.7 %copy-start.25 = (bf16[2,1024,128]{2,1,0:T(8,128)(2,1)S(1)}, bf16[2,1024,128]{2,1,0:T(8,128)(2,1)}, u32[]{:S(2)}) copy-start(bf16[2,1024,128]{2,1,0:T(8,128)(2,1)} %copy-done.24) | copy-start | bytes 1572868
  160.0 41.3 %copy-start.7 = (bf16[512,1024]{1,0:T(8,128)(2,1)S(1)}, bf16[512,1024]{1,0:T(8,128)(2,1)}, u32[]{:S(2)}) copy-start(bf16[512,1024]{1,0:T(8,128)(2,1)} %copy-done.6) | copy-start | bytes 3145732
  197.2 20.9 %collective-permute-start.8 = (bf16[2,1024,128]{2,1,0:T(8,128)(2,1)S(1)}, bf16[2,1024,128]{2,1,0:T(8,128)(2,1)S(1)}, u32[]{:S(2)}, u32[]{:S(2)}) collective-permute-start(bf16[2,1024,128]{2,1,0:T(8,128)(2,1)S(1)} %get-tuple-element.71.refs_8_), channel_id=1, source_target_pairs={{0,2},{1,3},{2,0},{3,1},{4,6},{5,7},{6,4},{7,5},{8,10},{9,11},{10,... | collective-permute-start | bytes 1572872 | tf_op jit(solution)/shard_map/ppermute | solution.py:332
  198.7 24.5 %collective-permute-start.10 = (bf16[2,1024,128]{2,1,0:T(8,128)(2,1)S(1)}, bf16[2,1024,128]{2,1,0:T(8,128)(2,1)S(1)}, u32[]{:S(2)}, u32[]{:S(2)}) collective-permute-start(bf16[2,1024,128]{2,1,0:T(8,128)(2,1)S(1)} %copy-done.25), channel_id=1, source_target_pairs={{0,2},{1,3},{2,0},{3,1},{4,6},{5,7},{6,4},{7,5},{8,10},{9,11},{10,... | collective-permute-start | bytes 1572872 | tf_op jit(solution)/shard_map/ppermute | solution.py:332
  199.2 35.2 %collective-permute-start.12 = (bf16[2,1024,128]{2,1,0:T(8,128)(2,1)S(1)}, bf16[2,1024,128]{2,1,0:T(8,128)(2,1)S(1)}, u32[]{:S(2)}, u32[]{:S(2)}) collective-permute-start(bf16[2,1024,128]{2,1,0:T(8,128)(2,1)S(1)} %collective-permute-done.11.refs_12_), channel_id=1, source_target_pairs={{0,2},{1,3},{2,0},{3,1},{4,6},{5,7},{6,4},{7,5},{8,10},{9,11},{10,... | collective-permute-start | bytes 1572872 | tf_op jit(solution)/shard_map/ppermute | solution.py:332
  200.7 45.0 %collective-permute-start.14 = (bf16[2,1024,128]{2,1,0:T(8,128)(2,1)S(1)}, bf16[2,1024,128]{2,1,0:T(8,128)(2,1)S(1)}, u32[]{:S(2)}, u32[]{:S(2)}) collective-permute-start(bf16[2,1024,128]{2,1,0:T(8,128)(2,1)S(1)} %collective-permute-done.13.refs_14_), channel_id=1, source_target_pairs={{0,2},{1,3},{2,0},{3,1},{4,6},{5,7},{6,4},{7,5},{8,10},{9,11},{10,... | collective-permute-start | bytes 1572872 | tf_op jit(solution)/shard_map/ppermute | solution.py:332
  216.6 80.0 %collective-permute-start.45 = (bf16[2,1024,128]{2,1,0:T(8,128)(2,1)S(1)}, bf16[2,1024,128]{2,1,0:T(8,128)(2,1)S(1)}, u32[]{:S(2)}, u32[]{:S(2)}) collective-permute-start(bf16[2,1024,128]{2,1,0:T(8,128)(2,1)S(1)} %get-tuple-element.48), channel_id=1, source_target_pairs={{0,2},{1,3},{2,0},{3,1},{4,6},{5,7},{6,4},{7,5},{8,10},{9,11},{10,... | collective-permute-start | bytes 1572872 | tf_op jit(solution)/shard_map/ppermute | solution.py:332
  218.1 116.2 %collective-permute-start.47 = (bf16[2,1024,128]{2,1,0:T(8,128)(2,1)S(1)}, bf16[2,1024,128]{2,1,0:T(8,128)(2,1)S(1)}, u32[]{:S(2)}, u32[]{:S(2)}) collective-permute-start(bf16[2,1024,128]{2,1,0:T(8,128)(2,1)S(1)} %get-tuple-element.50), channel_id=1, source_target_pairs={{0,2},{1,3},{2,0},{3,1},{4,6},{5,7},{6,4},{7,5},{8,10},{9,11},{10,... | collective-permute-start | bytes 1572872 | tf_op jit(solution)/shard_map/ppermute | solution.py:332
  223.2 74.1 %collective-permute-start.48 = (bf16[2,1024,128]{2,1,0:T(8,128)(2,1)S(1)}, bf16[2,1024,128]{2,1,0:T(8,128)(2,1)S(1)}, u32[]{:S(2)}, u32[]{:S(2)}) collective-permute-start(bf16[2,1024,128]{2,1,0:T(8,128)(2,1)S(1)} %get-tuple-element.52), channel_id=1, source_target_pairs={{0,2},{1,3},{2,0},{3,1},{4,6},{5,7},{6,4},{7,5},{8,10},{9,11},{10,... | collective-permute-start | bytes 1572872 | tf_op jit(solution)/shard_map/ppermute | solution.py:332
  234.5 64.6 %collective-permute-start.50 = (bf16[2,1024,128]{2,1,0:T(8,128)(2,1)S(1)}, bf16[2,1024,128]{2,1,0:T(8,128)(2,1)S(1)}, u32[]{:S(2)}, u32[]{:S(2)}) collective-permute-start(bf16[2,1024,128]{2,1,0:T(8,128)(2,1)S(1)} %get-tuple-element.54), channel_id=1, source_target_pairs={{0,2},{1,3},{2,0},{3,1},{4,6},{5,7},{6,4},{7,5},{8,10},{9,11},{10,... | collective-permute-start | bytes 1572872 | tf_op jit(solution)/shard_map/ppermute | solution.py:332
  264.5 17.0 %copy-start.23 = (bf16[2,1024,128]{2,1,0:T(8,128)(2,1)S(1)}, bf16[2,1024,128]{2,1,0:T(8,128)(2,1)}, u32[]{:S(2)}) copy-start(bf16[2,1024,128]{2,1,0:T(8,128)(2,1)} %copy-done.21) | copy-start | bytes 1572868
  264.5 17.0 %copy-start.28 = (bf16[2,1024,128]{2,1,0:T(8,128)(2,1)S(1)}, bf16[2,1024,128]{2,1,0:T(8,128)(2,1)}, u32[]{:S(2)}) copy-start(bf16[2,1024,128]{2,1,0:T(8,128)(2,1)} %copy-done.26) | copy-start | bytes 1572868
  279.9 21.9 %collective-permute-start.37 = (bf16[2,1024,128]{2,1,0:T(8,128)(2,1)S(1)}, bf16[2,1024,128]{2,1,0:T(8,128)(2,1)S(1)}, u32[]{:S(2)}, u32[]{:S(2)}) collective-permute-start(bf16[2,1024,128]{2,1,0:T(8,128)(2,1)S(1)} %get-tuple-element.39), channel_id=1, source_target_pairs={{0,2},{1,3},{2,0},{3,1},{4,6},{5,7},{6,4},{7,5},{8,10},{9,11},{10,... | collective-permute-start | bytes 1572872 | tf_op jit(solution)/shard_map/ppermute | solution.py:332
  296.6 72.4 %collective-permute-start.39 = (bf16[2,1024,128]{2,1,0:T(8,128)(2,1)S(1)}, bf16[2,1024,128]{2,1,0:T(8,128)(2,1)S(1)}, u32[]{:S(2)}, u32[]{:S(2)}) collective-permute-start(bf16[2,1024,128]{2,1,0:T(8,128)(2,1)S(1)} %get-tuple-element.41), channel_id=1, source_target_pairs={{0,2},{1,3},{2,0},{3,1},{4,6},{5,7},{6,4},{7,5},{8,10},{9,11},{10,... | collective-permute-start | bytes 1572872 | tf_op jit(solution)/shard_map/ppermute | solution.py:332
  297.3 27.0 %collective-permute-start.40 = (bf16[2,1024,128]{2,1,0:T(8,128)(2,1)S(1)}, bf16[2,1024,128]{2,1,0:T(8,128)(2,1)S(1)}, u32[]{:S(2)}, u32[]{:S(2)}) collective-permute-start(bf16[2,1024,128]{2,1,0:T(8,128)(2,1)S(1)} %get-tuple-element.43), channel_id=1, source_target_pairs={{0,2},{1,3},{2,0},{3,1},{4,6},{5,7},{6,4},{7,5},{8,10},{9,11},{10,... | collective-permute-start | bytes 1572872 | tf_op jit(solution)/shard_map/ppermute | solution.py:332
  299.0 35.1 %collective-permute-start.42 = (bf16[2,1024,128]{2,1,0:T(8,128)(2,1)S(1)}, bf16[2,1024,128]{2,1,0:T(8,128)(2,1)S(1)}, u32[]{:S(2)}, u32[]{:S(2)}) collective-permute-start(bf16[2,1024,128]{2,1,0:T(8,128)(2,1)S(1)} %get-tuple-element.45), channel_id=1, source_target_pairs={{0,2},{1,3},{2,0},{3,1},{4,6},{5,7},{6,4},{7,5},{8,10},{9,11},{10,... | collective-permute-start | bytes 1572872 | tf_op jit(solution)/shard_map/ppermute | solution.py:332
  301.9 103.0 %collective-permute-start.34 = (bf16[512,1024]{1,0:T(8,128)(2,1)S(1)}, bf16[512,1024]{1,0:T(8,128)(2,1)S(1)}, u32[]{:S(2)}, u32[]{:S(2)}) collective-permute-start(bf16[512,1024]{1,0:T(8,128)(2,1)S(1)} %get-tuple-element.37), channel_id=1, source_target_pairs={{0,1},{1,0},{2,3},{3,2},{4,5},{5,4},{6,7},{7,6},{8,9},{9,8},{10,11... | collective-permute-start | bytes 3145736 | tf_op jit(solution)/shard_map/ppermute | solution.py:332
  324.3 44.5 %collective-permute-start.46 = (bf16[2,1024,128]{2,1,0:T(8,128)(2,1)S(1)}, bf16[2,1024,128]{2,1,0:T(8,128)(2,1)S(1)}, u32[]{:S(2)}, u32[]{:S(2)}) collective-permute-start(bf16[2,1024,128]{2,1,0:T(8,128)(2,1)S(1)} %add_convert_fusion.6), channel_id=1, source_target_pairs={{0,16},{1,17},{2,18},{3,19},{4,20},{5,21},{6,22},{7,23},{8,24},{9,... | collective-permute-start | bytes 1572872 | tf_op jit(solution)/shard_map/ppermute | solution.py:332
  334.2 45.9 %collective-permute-start.38 = (bf16[2,1024,128]{2,1,0:T(8,128)(2,1)S(1)}, bf16[2,1024,128]{2,1,0:T(8,128)(2,1)S(1)}, u32[]{:S(2)}, u32[]{:S(2)}) collective-permute-start(bf16[2,1024,128]{2,1,0:T(8,128)(2,1)S(1)} %add_convert_fusion.9), channel_id=1, source_target_pairs={{0,16},{1,17},{2,18},{3,19},{4,20},{5,21},{6,22},{7,23},{8,24},{9,... | collective-permute-start | bytes 1572872 | tf_op jit(solution)/shard_map/ppermute | solution.py:332
  334.3 45.9 %collective-permute-start.41 = (bf16[2,1024,128]{2,1,0:T(8,128)(2,1)S(1)}, bf16[2,1024,128]{2,1,0:T(8,128)(2,1)S(1)}, u32[]{:S(2)}, u32[]{:S(2)}) collective-permute-start(bf16[2,1024,128]{2,1,0:T(8,128)(2,1)S(1)} %add_convert_fusion.8), channel_id=1, source_target_pairs={{0,24},{1,25},{2,26},{3,27},{4,28},{5,29},{6,30},{7,31},{8,16},{9,... | collective-permute-start | bytes 1572872 | tf_op jit(solution)/shard_map/ppermute | solution.py:332
  368.8 33.6 %collective-permute-start.43 = (bf16[2,1024,128]{2,1,0:T(8,128)(2,1)S(1)}, bf16[2,1024,128]{2,1,0:T(8,128)(2,1)S(1)}, u32[]{:S(2)}, u32[]{:S(2)}) collective-permute-start(bf16[2,1024,128]{2,1,0:T(8,128)(2,1)S(1)} %add_convert_fusion.7), channel_id=1, source_target_pairs={{0,8},{1,9},{2,10},{3,11},{4,12},{5,13},{6,14},{7,15},{8,0},{9,1},... | collective-permute-start | bytes 1572872 | tf_op jit(solution)/shard_map/ppermute | solution.py:332
  369.0 50.1 %collective-permute-start.31 = (bf16[512,1024]{1,0:T(8,128)(2,1)S(1)}, bf16[512,1024]{1,0:T(8,128)(2,1)S(1)}, u32[]{:S(2)}, u32[]{:S(2)}) collective-permute-start(bf16[512,1024]{1,0:T(8,128)(2,1)S(1)} %get-tuple-element.33), channel_id=1, source_target_pairs={{0,1},{1,0},{2,3},{3,2},{4,5},{5,4},{6,7},{7,6},{8,9},{9,8},{10,11... | collective-permute-start | bytes 3145736 | tf_op jit(solution)/shard_map/ppermute | solution.py:332
  380.1 64.2 %collective-permute-start.33 = (bf16[512,1024]{1,0:T(8,128)(2,1)S(1)}, bf16[512,1024]{1,0:T(8,128)(2,1)S(1)}, u32[]{:S(2)}, u32[]{:S(2)}) collective-permute-start(bf16[512,1024]{1,0:T(8,128)(2,1)S(1)} %get-tuple-element.35), channel_id=1, source_target_pairs={{0,1},{1,0},{2,3},{3,2},{4,5},{5,4},{6,7},{7,6},{8,9},{9,8},{10,11... | collective-permute-start | bytes 3145736 | tf_op jit(solution)/shard_map/ppermute | solution.py:332
  380.3 26.6 %collective-permute-start.49 = (bf16[2,1024,128]{2,1,0:T(8,128)(2,1)S(1)}, bf16[2,1024,128]{2,1,0:T(8,128)(2,1)S(1)}, u32[]{:S(2)}, u32[]{:S(2)}) collective-permute-start(bf16[2,1024,128]{2,1,0:T(8,128)(2,1)S(1)} %add_convert_fusion.5), channel_id=1, source_target_pairs={{0,24},{1,25},{2,26},{3,27},{4,28},{5,29},{6,30},{7,31},{8,16},{9,... | collective-permute-start | bytes 1572872 | tf_op jit(solution)/shard_map/ppermute | solution.py:332
  402.4 14.1 %collective-permute-start.51 = (bf16[2,1024,128]{2,1,0:T(8,128)(2,1)S(1)}, bf16[2,1024,128]{2,1,0:T(8,128)(2,1)S(1)}, u32[]{:S(2)}, u32[]{:S(2)}) collective-permute-start(bf16[2,1024,128]{2,1,0:T(8,128)(2,1)S(1)} %add_convert_fusion.4), channel_id=1, source_target_pairs={{0,8},{1,9},{2,10},{3,11},{4,12},{5,13},{6,14},{7,15},{8,0},{9,1},... | collective-permute-start | bytes 1572872 | tf_op jit(solution)/shard_map/ppermute | solution.py:332
  405.3 39.0 %collective-permute-start.35 = (bf16[512,1024]{1,0:T(8,128)(2,1)S(1)}, bf16[512,1024]{1,0:T(8,128)(2,1)S(1)}, u32[]{:S(2)}, u32[]{:S(2)}) collective-permute-start(bf16[512,1024]{1,0:T(8,128)(2,1)S(1)} %add_convert_fusion.2), channel_id=1, source_target_pairs={{0,4},{1,5},{2,6},{3,7},{4,0},{5,1},{6,2},{7,3},{8,12},{9,13},{10,... | collective-permute-start | bytes 3145736 | tf_op jit(solution)/shard_map/ppermute | solution.py:332
  406.9 49.8 %collective-permute-start.30 = (bf16[512,1024]{1,0:T(8,128)(2,1)S(1)}, bf16[512,1024]{1,0:T(8,128)(2,1)}, u32[]{:S(2)}, u32[]{:S(2)}) collective-permute-start(bf16[512,1024]{1,0:T(8,128)(2,1)S(1)} %get-tuple-element.31), channel_id=1, source_target_pairs={{0,1},{1,0},{2,3},{3,2},{4,5},{5,4},{6,7},{7,6},{8,9},{9,8},{10,11... | collective-permute-start | bytes 3145736 | tf_op jit(solution)/shard_map/ppermute | solution.py:332
  416.5 26.1 %collective-permute-start.44 = (bf16[2,1024,128]{2,1,0:T(8,128)(2,1)S(1)}, bf16[2,1024,128]{2,1,0:T(8,128)(2,1)S(1)}, u32[]{:S(2)}, u32[]{:S(2)}) collective-permute-start(bf16[2,1024,128]{2,1,0:T(8,128)(2,1)S(1)} %pad_maximum_fusion.1), channel_id=1, source_target_pairs={{0,4},{1,5},{2,6},{3,7},{4,0},{5,1},{6,2},{7,3},{8,12},{9,13},{10,... | collective-permute-start | bytes 1572872 | tf_op jit(solution)/shard_map/ppermute | solution.py:332
  419.3 34.6 %collective-permute-start.52 = (bf16[2,1024,128]{2,1,0:T(8,128)(2,1)}, bf16[2,1024,128]{2,1,0:T(8,128)(2,1)}, u32[]{:S(2)}, u32[]{:S(2)}) collective-permute-start(bf16[2,1024,128]{2,1,0:T(8,128)(2,1)} %pad_maximum_fusion.2), channel_id=1, source_target_pairs={{0,4},{1,5},{2,6},{3,7},{4,0},{5,1},{6,2},{7,3},{8,12},{9,13},{10,... | collective-permute-start | bytes 1572872 | tf_op jit(solution)/shard_map/ppermute | solution.py:332
  442.6 32.3 %collective-permute-start.32 = (bf16[512,1024]{1,0:T(8,128)(2,1)}, bf16[512,1024]{1,0:T(8,128)(2,1)}, u32[]{:S(2)}, u32[]{:S(2)}) collective-permute-start(bf16[512,1024]{1,0:T(8,128)(2,1)} %add_convert_fusion.3), channel_id=1, source_target_pairs={{0,4},{1,5},{2,6},{3,7},{4,0},{5,1},{6,2},{7,3},{8,12},{9,13},{10,... | collective-permute-start | bytes 3145736 | tf_op jit(solution)/shard_map/ppermute | solution.py:332
  445.9 29.0 %collective-permute-start.36 = (bf16[512,1024]{1,0:T(8,128)(2,1)}, bf16[512,1024]{1,0:T(8,128)(2,1)}, u32[]{:S(2)}, u32[]{:S(2)}) collective-permute-start(bf16[512,1024]{1,0:T(8,128)(2,1)} %add_convert_fusion.1), channel_id=1, source_target_pairs={{0,8},{1,9},{2,10},{3,11},{4,12},{5,13},{6,14},{7,15},{8,0},{9,1},... | collective-permute-start | bytes 3145736 | tf_op jit(solution)/shard_map/ppermute | solution.py:332
  (25 other events, 112.1 us)
where the time goes:
time: 479 us
  waiting for transfers between devices  308 us (64%)
  Pallas kernels  73.4 us (15%)
  starting transfers between devices  50.9 us (11%)
  local copies, waits for them, and re-layouts  30 us (6%)
  other arithmetic  15.1 us (3%)
    ppermute x53, waiting for transfers between devices, send(): return lax.ppermute(value, AXES, perm)  308 us
    pallas_call x5, Pallas kernels, call(): pl.pallas_call(body, out_shape=[jax.ShapeDtypeStruct(o, BF) for o in outs...  73.4 us
    ppermute x53, starting transfers between devices, send(): return lax.ppermute(value, AXES, perm)  50.9 us
    unnamed x74, local copies, waits for them, and re-layouts  25.1 us
  transfers between devices with their start and end apart: 53, of which 25 were waited for; matrix products, arithmetic and copies ran while one was open for 3% of the time, Pallas kernels for 15%

commit v1 on v0

--- a/solution.py
+++ b/solution.py
@@ -337,9 +337,14 @@
         pieces = (value, side, near, send(near, 2))
         return [[p] + [send(p, 0, c) for c in range(1, m)] for p in pieces]
 
-    def gather_weights(w):
-        w = w.reshape(2, 2, width, d_rows)
-        mine, theirs = pick(w, 0, py), send(pick(w, 0, 1 - py), 2)
+    def gather_weights(tag, w):
+        def half(y):
+            if tag == "u":
+                return pick(w.reshape(d_rows, 2, ff // 2), 1, y).T.reshape(2, width, d_rows)
+            return pick(w.reshape(2, 2, width, d_rows), 0, y)
+
+        theirs = send(half(1 - py), 2)
+        mine = half(py)
         both = jnp.stack([mine, theirs])
         halves = [pick(both, 1, zl), pick(both, 1, 1 - zl)]
         pieces = []
@@ -352,9 +357,9 @@
         return [a for row in lists for a in row]
 
     x4 = gather_tokens(x)
-    wu = gather_weights(up.T)
+    wu = gather_weights("u", up)
     dy4 = gather_tokens(dy)
-    wd = gather_weights(down)
+    wd = gather_weights("d", down)
     every = 4 * rows
     hid, feats = (4, width, rows), n * d_rows
     nw, nt = 4 * planes, 4 * m
@@ -427,7 +432,8 @@
             own[p] = own[p] + send(dx[4 * c + p], 0, c).astype(F32)
     far = own[2] + send(own[3].astype(BF), 2).astype(F32)
     near = own[0] + send(own[1].astype(BF), 2).astype(F32)
-    input_grad = (near + send(far.astype(BF), 4).astype(F32)).astype(BF)
+    far = send(far.astype(BF), 4)
+    input_grad = (near + far.astype(F32)).astype(BF)
     return input_grad, up_grad, down_grad
 
 

time: 479 us -> 478 us (level)
  no operation moved by 1% of the time
where the time goes in v1:
time: 478 us; the launch traced here: 477 us
  waiting for transfers between devices  309 us (65%)
  Pallas kernels  73.3 us (15%)
  starting transfers between devices  50.9 us (11%)
  local copies, waits for them, and re-layouts  28.3 us (6%)
  other arithmetic  15.1 us (3%)
    ppermute x53, waiting for transfers between devices, send(): return lax.ppermute(value, AXES, perm)  309 us
    pallas_call x5, Pallas kernels, call(): pl.pallas_call(body, out_shape=[jax.ShapeDtypeStruct(o, BF) for o in outs...  73.3 us
    ppermute x53, starting transfers between devices, send(): return lax.ppermute(value, AXES, perm)  50.9 us
    unnamed x74, local copies, waits for them, and re-layouts  26.3 us
  transfers between devices with their start and end apart: 53, of which 25 were waited for; matrix products, arithmetic and copies ran while one was open for 3% of the time, Pallas kernels for 15%

profile of v1, /device:TPU:0, one launch (start us, length us, event | category | flops | bytes accessed | tf_op | source)
XLA Modules:
  0.0 477.5 jit_solution(13272146412176214776)
XLA Ops:
  0.7 1.7 copy.14
  3.3 3.0 collective-permute-start.22
  7.3 11.9 %collective-permute-done.22 = bf16[2,1024,128]{2,1,0:T(8,128)(2,1)S(1)} collective-permute-done((bf16[2,1024,128]{2,1,0:T(8,128)(2,1)}, bf16[2,1024,128]{2,1,0:T(8,128)(2,1)S(1)}, u32[]{:S(2)}, u32[]{:S(2)}) %collective-permute-start.22) | collective-permute-done | bytes 524320 | tf_op jit(solution)/shard_map/ppermute | solution.py:332
  19.3 2.1 collective-permute-start.24
  21.6 3.0 collective-permute-start.26
  25.9 3.9 collective-permute-done.7
  29.7 1.7 collective-permute-start.16
  31.5 13.9 %collective-permute-done.24.refs_10_.refs_3_ = bf16[2,1024,128]{2,1,0:T(8,128)(2,1)S(1)} collective-permute-done((bf16[2,1024,128]{2,1,0:T(8,128)(2,1)S(1)}, bf16[2,1024,128]{2,1,0:T(8,128)(2,1)S(1)}, u32[]{:S(2)}, u32[]{:S(2)}) %collective-permute-start.24) | collective-permute-done | bytes 524320 | tf_op jit(solution)/shard_map/ppermute | solution.py:332
  45.3 1.4 collective-permute-start.23
  46.8 20.7 %collective-permute-done.26.refs_12_.refs_5_ = bf16[2,1024,128]{2,1,0:T(8,128)(2,1)S(1)} collective-permute-done((bf16[2,1024,128]{2,1,0:T(8,128)(2,1)S(1)}, bf16[2,1024,128]{2,1,0:T(8,128)(2,1)S(1)}, u32[]{:S(2)}, u32[]{:S(2)}) %collective-permute-start.26) | collective-permute-done | bytes 524320 | tf_op jit(solution)/shard_map/ppermute | solution.py:332
  67.5 11.8 %collective-permute-done.28.refs_14_.refs_7_ = bf16[2,1024,128]{2,1,0:T(8,128)(2,1)S(1)} collective-permute-done((bf16[2,1024,128]{2,1,0:T(8,128)(2,1)S(1)}, bf16[2,1024,128]{2,1,0:T(8,128)(2,1)S(1)}, u32[]{:S(2)}, u32[]{:S(2)}) %collective-permute-start.28) | collective-permute-done | bytes 524320 | tf_op jit(solution)/shard_map/ppermute | solution.py:332
  80.2 1.5 collective-permute-start.1
  84.5 2.0 collective-permute-start.9
  86.4 19.1 %collective-permute-done.3.refs_4_ = bf16[512,1024]{1,0:T(8,128)(2,1)} collective-permute-done((bf16[512,1024]{1,0:T(8,128)(2,1)S(1)}, bf16[512,1024]{1,0:T(8,128)(2,1)}, u32[]{:S(2)}, u32[]{:S(2)}) %collective-permute-start.3) | collective-permute-done | bytes 1048608 | tf_op jit(solution)/shard_map/ppermute | solution.py:332
  105.5 1.5 collective-permute-start.25
  108.8 3.6 collective-permute-done.9.refs_10_
  112.5 1.5 collective-permute-start.5
  114.0 2.7 collective-permute-done.25.refs_11_.refs_4_
  117.5 11.3 %collective-permute-done.20.refs_6_ = bf16[512,1024]{1,0:T(8,128)(2,1)} collective-permute-done((bf16[512,1024]{1,0:T(8,128)(2,1)S(1)}, bf16[512,1024]{1,0:T(8,128)(2,1)}, u32[]{:S(2)}, u32[]{:S(2)}) %collective-permute-start.20) | collective-permute-done | bytes 1048608 | tf_op jit(solution)/shard_map/ppermute | solution.py:332
  129.6 1.5 collective-permute-start.29
  131.1 12.8 %collective-permute-done.29.refs_15_.refs_8_ = bf16[2,1024,128]{2,1,0:T(8,128)(2,1)S(1)} collective-permute-done((bf16[2,1024,128]{2,1,0:T(8,128)(2,1)S(1)}, bf16[2,1024,128]{2,1,0:T(8,128)(2,1)S(1)}, u32[]{:S(2)}, u32[]{:S(2)}) %collective-permute-start.29) | collective-permute-done | bytes 524320 | tf_op jit(solution)/shard_map/ppermute | solution.py:332
  146.5 1.4 collective-permute-start.13
  147.9 2.0 collective-permute-start.11
  158.8 15.2 %shard_map.67 = (bf16[4,1024,512]{2,1,0:T(8,128)(2,1)S(1)}, bf16[4,1024,512]{2,1,0:T(8,128)(2,1)S(1)}) custom-call(s32[1]{0:T(128)} %bitcast.base_ref, bf16[512,1024]{1,0:T(8,128)(2,1)} %refs_0_.6, bf16[512,1024]{1,0:T(8,128)(2,1)S(1)} %copy-done.4, bf16[512,1024]{1,0:T(8,128)(2,1)} %collective-permute-done.16.refs_2_, ...), custom_call_target="tpu_custom_call" | custom-call | flops 8589934592 | bytes 20971524 | tf_op jit(solution)/shard_map/pallas_call | solution.py:141
  174.0 22.0 %collective-permute-done.11.refs_12_ = bf16[2,1024,128]{2,1,0:T(8,128)(2,1)S(1)} collective-permute-done((bf16[2,1024,128]{2,1,0:T(8,128)(2,1)S(1)}, bf16[2,1024,128]{2,1,0:T(8,128)(2,1)S(1)}, u32[]{:S(2)}, u32[]{:S(2)}) %collective-permute-start.11) | collective-permute-done | bytes 524320 | tf_op jit(solution)/shard_map/ppermute | solution.py:332
  196.0 1.5 collective-permute-start.8
  198.1 1.5 collective-permute-start.12
  200.1 15.3 %shard_map.71 = (bf16[2,1024,128]{2,1,0:T(8,128)(2,1)S(1)}, bf16[2,1024,128]{2,1,0:T(8,128)(2,1)S(1)}, bf16[2,1024,128]{2,1,0:T(8,128)(2,1)S(1)}, bf16[2,1024,12...) custom-call(s32[1]{0:T(128)} %bitcast.base_ref, ...), custom_call_target="tpu_custom_call" | custom-call | flops 8589934592 | bytes 16777220 | tf_op jit(solution)/shard_map/pallas_call | solution.py:141
  215.4 1.5 collective-permute-start.45
  217.5 4.5 collective-permute-done.10.refs_11_
  222.1 1.5 collective-permute-start.48
  223.5 9.7 %collective-permute-done.12.refs_13_ = bf16[2,1024,128]{2,1,0:T(8,128)(2,1)S(1)} collective-permute-done((bf16[2,1024,128]{2,1,0:T(8,128)(2,1)S(1)}, bf16[2,1024,128]{2,1,0:T(8,128)(2,1)S(1)}, u32[]{:S(2)}, u32[]{:S(2)}) %collective-permute-start.12) | collective-permute-done | bytes 524320 | tf_op jit(solution)/shard_map/ppermute | solution.py:332
  233.3 1.5 collective-permute-start.50
  234.8 9.7 %collective-permute-done.14.refs_15_ = bf16[2,1024,128]{2,1,0:T(8,128)(2,1)S(1)} collective-permute-done((bf16[2,1024,128]{2,1,0:T(8,128)(2,1)S(1)}, bf16[2,1024,128]{2,1,0:T(8,128)(2,1)S(1)}, u32[]{:S(2)}, u32[]{:S(2)}) %collective-permute-start.14) | collective-permute-done | bytes 524320 | tf_op jit(solution)/shard_map/ppermute | solution.py:332
  244.5 14.6 %shard_map.68.refs_0_.refs_8_ = bf16[4,1024,512]{2,1,0:T(8,128)(2,1)S(1)} custom-call(s32[1]{0:T(128)} %bitcast.base_ref, bf16[512,1024]{1,0:T(8,128)(2,1)S(1)} %copy-done, bf16[512,1024]{1,0:T(8,128)(2,1)S(1)} %copy-done.7, bf16[512,1024]{1,0:T(8,128)(2,1)} %collective-permute-done.1.refs_2_, bf16[512,1024]{1,0:T(8,128)(2,1)} %collective-permute-done.2.refs_3_, ...), custom_call_target="tpu_custom_call" | custom-call | flops 8589934592 | bytes 20971524 | tf_op jit(solution)/shard_map/pallas_call | solution.py:141
  259.1 2.0 copy-done.29
  261.2 2.2 copy-done.30
  263.4 15.4 %shard_map.70 = (bf16[2,1024,128]{2,1,0:T(8,128)(2,1)S(1)}, bf16[2,1024,128]{2,1,0:T(8,128)(2,1)S(1)}, bf16[2,1024,128]{2,1,0:T(8,128)(2,1)S(1)}, bf16[2,1024,12...) custom-call(s32[1]{0:T(128)} %bitcast.base_ref, ...), custom_call_target="tpu_custom_call" | custom-call | flops 8589934592 | bytes 16777220 | tf_op jit(solution)/shard_map/pallas_call | solution.py:141
  278.8 1.6 collective-permute-start.37
  280.4 2.2 copy-done.31
  282.5 12.8 %shard_map.69 = (bf16[512,1024]{1,0:T(8,128)(2,1)S(1)}, bf16[512,1024]{1,0:T(8,128)(2,1)S(1)}, bf16[512,1024]{1,0:T(8,128)(2,1)S(1)}, bf16[512,1024]{1,0:T(8,128...) custom-call(s32[1]{0:T(128)} %bitcast.base_ref, ...), custom_call_target="tpu_custom_call" | custom-call | flops 8589934592 | bytes 16777220 | tf_op jit(solution)/shard_map/pallas_call | solution.py:141
  296.2 1.6 collective-permute-start.40
  298.6 2.1 collective-permute-done.37
  300.8 22.3 %collective-permute-done.40 = bf16[2,1024,128]{2,1,0:T(8,128)(2,1)S(1)} collective-permute-done((bf16[2,1024,128]{2,1,0:T(8,128)(2,1)S(1)}, bf16[2,1024,128]{2,1,0:T(8,128)(2,1)S(1)}, u32[]{:S(2)}, u32[]{:S(2)}) %collective-permute-start.40) | collective-permute-done | bytes 524320 | tf_op jit(solution)/shard_map/ppermute | solution.py:332
  323.3 9.7 %collective-permute-done.42 = bf16[2,1024,128]{2,1,0:T(8,128)(2,1)S(1)} collective-permute-done((bf16[2,1024,128]{2,1,0:T(8,128)(2,1)S(1)}, bf16[2,1024,128]{2,1,0:T(8,128)(2,1)S(1)}, u32[]{:S(2)}, u32[]{:S(2)}) %collective-permute-start.42) | collective-permute-done | bytes 524320 | tf_op jit(solution)/shard_map/ppermute | solution.py:332
  334.5 33.2 %collective-permute-done.46 = bf16[2,1024,128]{2,1,0:T(8,128)(2,1)S(1)} collective-permute-done((bf16[2,1024,128]{2,1,0:T(8,128)(2,1)S(1)}, bf16[2,1024,128]{2,1,0:T(8,128)(2,1)S(1)}, u32[]{:S(2)}, u32[]{:S(2)}) %collective-permute-start.46) | collective-permute-done | bytes 524320 | tf_op jit(solution)/shard_map/ppermute | solution.py:332
  367.9 11.0 %collective-permute-done.38 = bf16[2,1024,128]{2,1,0:T(8,128)(2,1)S(1)} collective-permute-done((bf16[2,1024,128]{2,1,0:T(8,128)(2,1)S(1)}, bf16[2,1024,128]{2,1,0:T(8,128)(2,1)S(1)}, u32[]{:S(2)}, u32[]{:S(2)}) %collective-permute-start.38) | collective-permute-done | bytes 524320 | tf_op jit(solution)/shard_map/ppermute | solution.py:332
  379.1 2.6 collective-permute-start.49
  381.7 19.5 %collective-permute-done.43 = bf16[2,1024,128]{2,1,0:T(8,128)(2,1)S(1)} collective-permute-done((bf16[2,1024,128]{2,1,0:T(8,128)(2,1)S(1)}, bf16[2,1024,128]{2,1,0:T(8,128)(2,1)S(1)}, u32[]{:S(2)}, u32[]{:S(2)}) %collective-permute-start.43) | collective-permute-done | bytes 524320 | tf_op jit(solution)/shard_map/ppermute | solution.py:332
  401.2 2.3 collective-permute-start.51
  404.1 1.6 collective-permute-start.35
  405.8 9.5 %collective-permute-done.51 = bf16[2,1024,128]{2,1,0:T(8,128)(2,1)S(1)} collective-permute-done((bf16[2,1024,128]{2,1,0:T(8,128)(2,1)S(1)}, bf16[2,1024,128]{2,1,0:T(8,128)(2,1)S(1)}, u32[]{:S(2)}, u32[]{:S(2)}) %collective-permute-start.51) | collective-permute-done | bytes 524320 | tf_op jit(solution)/shard_map/ppermute | solution.py:332
  415.3 1.5 collective-permute-start.44
  418.6 1.4 add_convert_fusion.3
  420.0 21.4 %collective-permute-done.44 = bf16[2,1024,128]{2,1,0:T(8,128)(2,1)S(1)} collective-permute-done((bf16[2,1024,128]{2,1,0:T(8,128)(2,1)S(1)}, bf16[2,1024,128]{2,1,0:T(8,128)(2,1)S(1)}, u32[]{:S(2)}, u32[]{:S(2)}) %collective-permute-start.44) | collective-permute-done | bytes 524320 | tf_op jit(solution)/shard_map/ppermute | solution.py:332
  441.4 1.5 collective-permute-start.32
  443.1 1.6 add_convert_fusion.1
  444.7 1.5 maximum_bitcast_fusion
  446.2 2.9 copy.19
  449.1 3.7 collective-permute-done.52
  452.8 1.4 select_bitcast_fusion.3
  454.1 1.5 pad_maximum_fusion
  455.6 18.1 %collective-permute-done.32 = bf16[512,1024]{1,0:T(8,128)(2,1)} collective-permute-done((bf16[512,1024]{1,0:T(8,128)(2,1)}, bf16[512,1024]{1,0:T(8,128)(2,1)}, u32[]{:S(2)}, u32[]{:S(2)}) %collective-permute-start.32) | collective-permute-done | bytes 1048608 | tf_op jit(solution)/shard_map/ppermute | solution.py:332
  473.7 3.7 add_convert_fusion
  (149 shorter events, 30.0 us)
Async XLA Ops:
  3.3 16.0 %collective-permute-start.22 = (bf16[2,1024,128]{2,1,0:T(8,128)(2,1)}, bf16[2,1024,128]{2,1,0:T(8,128)(2,1)S(1)}, u32[]{:S(2)}, u32[]{:S(2)}) collective-permute-start(bf16[2,1024,128]{2,1,0:T(8,128)(2,1)} %bitcast.12), channel_id=1, source_target_pairs={{0,4},{1,5},{2,6},{3,7},{4,0},{5,1},{6,2},{7,3},{8,12},{9,13},{10,... | collective-permute-start | bytes 1572872 | tf_op jit(solution)/shard_map/ppermute | solution.py:332
  6.3 73.1 %copy-start = (bf16[512,1024]{1,0:T(8,128)(2,1)S(1)}, bf16[512,1024]{1,0:T(8,128)(2,1)}, u32[]{:S(2)}) copy-start(bf16[512,1024]{1,0:T(8,128)(2,1)} %refs_0_.7) | copy-start | bytes 3145732
  7.3 22.4 %collective-permute-start.7 = (bf16[2,1024,128]{2,1,0:T(8,128)(2,1)}, bf16[2,1024,128]{2,1,0:T(8,128)(2,1)}, u32[]{:S(2)}, u32[]{:S(2)}) collective-permute-start(bf16[2,1024,128]{2,1,0:T(8,128)(2,1)} %get-tuple-element.78), channel_id=1, source_target_pairs={{0,4},{1,5},{2,6},{3,7},{4,0},{5,1},{6,2},{7,3},{8,12},{9,13},{10,... | collective-permute-start | bytes 1572872 | tf_op jit(solution)/shard_map/ppermute | solution.py:332
  7.3 75.0 %copy-start.33 = (bf16[1,2,1024,128]{3,2,0,1:T(8,128)(2,1)S(1)}, bf16[1,2,1024,128]{3,2,0,1:T(8,128)(2,1)}, u32[]{:S(2)}) copy-start(bf16[1,2,1024,128]{3,2,0,1:T(8,128)(2,1)} %get-tuple-element.79) | copy-start | bytes 1572868
  19.3 26.0 %collective-permute-start.24 = (bf16[2,1024,128]{2,1,0:T(8,128)(2,1)S(1)}, bf16[2,1024,128]{2,1,0:T(8,128)(2,1)S(1)}, u32[]{:S(2)}, u32[]{:S(2)}) collective-permute-start(bf16[2,1024,128]{2,1,0:T(8,128)(2,1)S(1)} %get-tuple-element.72), channel_id=1, source_target_pairs={{0,8},{1,9},{2,10},{3,11},{4,12},{5,13},{6,14},{7,15},{8,0},{9,1},... | collective-permute-start | bytes 1572872 | tf_op jit(solution)/shard_map/ppermute | solution.py:332
  21.5 60.2 %collective-permute-start.18 = (bf16[512,1024]{1,0:T(8,128)(2,1)}, bf16[512,1024]{1,0:T(8,128)(2,1)S(1)}, u32[]{:S(2)}, u32[]{:S(2)}) collective-permute-start(bf16[512,1024]{1,0:T(8,128)(2,1)} %refs_0_.6), channel_id=1, source_target_pairs={{0,8},{1,9},{2,10},{3,11},{4,12},{5,13},{6,14},{7,15},{8,0},{9,1},... | collective-permute-start | bytes 3145736 | tf_op jit(solution)/shard_map/ppermute | solution.py:332
  21.6 45.9 %collective-permute-start.26 = (bf16[2,1024,128]{2,1,0:T(8,128)(2,1)S(1)}, bf16[2,1024,128]{2,1,0:T(8,128)(2,1)S(1)}, u32[]{:S(2)}, u32[]{:S(2)}) collective-permute-start(bf16[2,1024,128]{2,1,0:T(8,128)(2,1)S(1)} %get-tuple-element.73.refs_8_.refs_1_), channel_id=1, source_target_pairs={{0,16},{1,17},{2,18},{3,19},{4,20},{5,21},{6,22},{7,23},{8,24},{9,... | collective-permute-start | bytes 1572872 | tf_op jit(solution)/shard_map/ppermute | solution.py:332
  24.5 54.8 %collective-permute-start.28 = (bf16[2,1024,128]{2,1,0:T(8,128)(2,1)S(1)}, bf16[2,1024,128]{2,1,0:T(8,128)(2,1)S(1)}, u32[]{:S(2)}, u32[]{:S(2)}) collective-permute-start(bf16[2,1024,128]{2,1,0:T(8,128)(2,1)S(1)} %get-tuple-element.72), channel_id=1, source_target_pairs={{0,24},{1,25},{2,26},{3,27},{4,28},{5,29},{6,30},{7,31},{8,16},{9,... | collective-permute-start | bytes 1572872 | tf_op jit(solution)/shard_map/ppermute | solution.py:332
  29.7 52.0 %collective-permute-start.16 = (bf16[512,1024]{1,0:T(8,128)(2,1)}, bf16[512,1024]{1,0:T(8,128)(2,1)}, u32[]{:S(2)}, u32[]{:S(2)}) collective-permute-start(bf16[512,1024]{1,0:T(8,128)(2,1)} %refs_0_.6), channel_id=1, source_target_pairs={{0,4},{1,5},{2,6},{3,7},{4,0},{5,1},{6,2},{7,3},{8,12},{9,13},{10,... | collective-permute-start | bytes 3145736 | tf_op jit(solution)/shard_map/ppermute | solution.py:332
  45.3 34.0 %collective-permute-start.23 = (bf16[2,1024,128]{2,1,0:T(8,128)(2,1)S(1)}, bf16[2,1024,128]{2,1,0:T(8,128)(2,1)S(1)}, u32[]{:S(2)}, u32[]{:S(2)}) collective-permute-start(bf16[2,1024,128]{2,1,0:T(8,128)(2,1)S(1)} %get-tuple-element.73.refs_8_.refs_1_), channel_id=1, source_target_pairs={{0,2},{1,3},{2,0},{3,1},{4,6},{5,7},{6,4},{7,5},{8,10},{9,11},{10,... | collective-permute-start | bytes 1572872 | tf_op jit(solution)/shard_map/ppermute | solution.py:332
  67.5 106.5 %copy-start.10 = (bf16[2,1024,128]{2,1,0:T(8,128)(2,1)}, bf16[2,1024,128]{2,1,0:T(8,128)(2,1)S(1)}, u32[]{:S(2)}) copy-start(bf16[2,1024,128]{2,1,0:T(8,128)(2,1)S(1)} %collective-permute-done.26.refs_12_.refs_5_) | copy-start | bytes 1572868
  67.5 15.9 %collective-permute-start.15 = (bf16[512,1024]{1,0:T(8,128)(2,1)}, bf16[512,1024]{1,0:T(8,128)(2,1)S(1)}, u32[]{:S(2)}, u32[]{:S(2)}) collective-permute-start(bf16[512,1024]{1,0:T(8,128)(2,1)} %refs_0_.6), channel_id=1, source_target_pairs={{0,1},{1,0},{2,3},{3,2},{4,5},{5,4},{6,7},{7,6},{8,9},{9,8},{10,11... | collective-permute-start | bytes 3145736 | tf_op jit(solution)/shard_map/ppermute | solution.py:332
  79.4 65.4 %copy-start.12 = (bf16[2,1024,128]{2,1,0:T(8,128)(2,1)}, bf16[2,1024,128]{2,1,0:T(8,128)(2,1)S(1)}, u32[]{:S(2)}) copy-start(bf16[2,1024,128]{2,1,0:T(8,128)(2,1)S(1)} %collective-permute-done.28.refs_14_.refs_7_) | copy-start | bytes 1572868
  79.4 26.1 %collective-permute-start.3 = (bf16[512,1024]{1,0:T(8,128)(2,1)S(1)}, bf16[512,1024]{1,0:T(8,128)(2,1)}, u32[]{:S(2)}, u32[]{:S(2)}) collective-permute-start(bf16[512,1024]{1,0:T(8,128)(2,1)S(1)} %copy-done), channel_id=1, source_target_pairs={{0,8},{1,9},{2,10},{3,11},{4,12},{5,13},{6,14},{7,15},{8,0},{9,1},... | collective-permute-start | bytes 3145736 | tf_op jit(solution)/shard_map/ppermute | solution.py:332
  80.2 26.8 %collective-permute-start.1 = (bf16[512,1024]{1,0:T(8,128)(2,1)S(1)}, bf16[512,1024]{1,0:T(8,128)(2,1)}, u32[]{:S(2)}, u32[]{:S(2)}) collective-permute-start(bf16[512,1024]{1,0:T(8,128)(2,1)S(1)} %copy-done), channel_id=1, source_target_pairs={{0,4},{1,5},{2,6},{3,7},{4,0},{5,1},{6,2},{7,3},{8,12},{9,13},{10,... | collective-permute-start | bytes 3145736 | tf_op jit(solution)/shard_map/ppermute | solution.py:332
  81.7 26.1 %copy-start.1 = (bf16[512,1024]{1,0:T(8,128)(2,1)}, bf16[512,1024]{1,0:T(8,128)(2,1)S(1)}, u32[]{:S(2)}) copy-start(bf16[512,1024]{1,0:T(8,128)(2,1)S(1)} %collective-permute-done.18.refs_4_) | copy-start | bytes 3145732
  81.7 26.1 %collective-permute-start = (bf16[512,1024]{1,0:T(8,128)(2,1)S(1)}, bf16[512,1024]{1,0:T(8,128)(2,1)S(1)}, u32[]{:S(2)}, u32[]{:S(2)}) collective-permute-start(bf16[512,1024]{1,0:T(8,128)(2,1)S(1)} %copy-done), channel_id=1, source_target_pairs={{0,1},{1,0},{2,3},{3,2},{4,5},{5,4},{6,7},{7,6},{8,9},{9,8},{10,11... | collective-permute-start | bytes 3145736 | tf_op jit(solution)/shard_map/ppermute | solution.py:332
  81.7 47.1 %collective-permute-start.20 = (bf16[512,1024]{1,0:T(8,128)(2,1)S(1)}, bf16[512,1024]{1,0:T(8,128)(2,1)}, u32[]{:S(2)}, u32[]{:S(2)}) collective-permute-start(bf16[512,1024]{1,0:T(8,128)(2,1)S(1)} %collective-permute-done.18.refs_4_), channel_id=1, source_target_pairs={{0,4},{1,5},{2,6},{3,7},{4,0},{5,1},{6,2},{7,3},{8,12},{9,13},{10,... | collective-permute-start | bytes 3145736 | tf_op jit(solution)/shard_map/ppermute | solution.py:332
  83.4 63.1 %copy-start.35 = (bf16[2,1024,128]{2,1,0:T(8,128)(2,1)}, bf16[2,1024,128]{2,1,0:T(8,128)(2,1)S(1)}, u32[]{:S(2)}) copy-start(bf16[2,1024,128]{2,1,0:T(8,128)(2,1)S(1)} %get-tuple-element.76) | copy-start | bytes 1572868
  84.5 28.0 %collective-permute-start.9 = (bf16[2,1024,128]{2,1,0:T(8,128)(2,1)S(1)}, bf16[2,1024,128]{2,1,0:T(8,128)(2,1)S(1)}, u32[]{:S(2)}, u32[]{:S(2)}) collective-permute-start(bf16[2,1024,128]{2,1,0:T(8,128)(2,1)S(1)} %get-tuple-element.76), channel_id=1, source_target_pairs={{0,8},{1,9},{2,10},{3,11},{4,12},{5,13},{6,14},{7,15},{8,0},{9,1},... | collective-permute-start | bytes 1572872 | tf_op jit(solution)/shard_map/ppermute | solution.py:332
  105.5 11.2 %collective-permute-start.25 = (bf16[2,1024,128]{2,1,0:T(8,128)(2,1)S(1)}, bf16[2,1024,128]{2,1,0:T(8,128)(2,1)S(1)}, u32[]{:S(2)}, u32[]{:S(2)}) collective-permute-start(bf16[2,1024,128]{2,1,0:T(8,128)(2,1)S(1)} %collective-permute-done.24.refs_10_.refs_3_), channel_id=1, source_target_pairs={{0,2},{1,3},{2,0},{3,1},{4,6},{5,7},{6,4},{7,5},{8,10},{9,11},{10,... | collective-permute-start | bytes 1572872 | tf_op jit(solution)/shard_map/ppermute | solution.py:332
  107.0 21.8 %collective-permute-start.27 = (bf16[2,1024,128]{2,1,0:T(8,128)(2,1)S(1)}, bf16[2,1024,128]{2,1,0:T(8,128)(2,1)S(1)}, u32[]{:S(2)}, u32[]{:S(2)}) collective-permute-start(bf16[2,1024,128]{2,1,0:T(8,128)(2,1)S(1)} %collective-permute-done.26.refs_12_.refs_5_), channel_id=1, source_target_pairs={{0,2},{1,3},{2,0},{3,1},{4,6},{5,7},{6,4},{7,5},{8,10},{9,11},{10,... | collective-permute-start | bytes 1572872 | tf_op jit(solution)/shard_map/ppermute | solution.py:332
  108.8 36.0 %collective-permute-start.19 = (bf16[512,1024]{1,0:T(8,128)(2,1)S(1)}, bf16[512,1024]{1,0:T(8,128)(2,1)S(1)}, u32[]{:S(2)}, u32[]{:S(2)}) collective-permute-start(bf16[512,1024]{1,0:T(8,128)(2,1)S(1)} %collective-permute-done.18.refs_4_), channel_id=1, source_target_pairs={{0,1},{1,0},{2,3},{3,2},{4,5},{5,4},{6,7},{7,6},{8,9},{9,8},{10,11... | collective-permute-start | bytes 3145736 | tf_op jit(solution)/shard_map/ppermute | solution.py:332
  112.5 33.8 %copy-start.24 = (bf16[2,1024,128]{2,1,0:T(8,128)(2,1)}, bf16[2,1024,128]{2,1,0:T(8,128)(2,1)S(1)}, u32[]{:S(2)}) copy-start(bf16[2,1024,128]{2,1,0:T(8,128)(2,1)S(1)} %collective-permute-done.9.refs_10_) | copy-start | bytes 1572868
  112.5 34.0 %collective-permute-start.5 = (bf16[512,1024]{1,0:T(8,128)(2,1)}, bf16[512,1024]{1,0:T(8,128)(2,1)}, u32[]{:S(2)}, u32[]{:S(2)}) collective-permute-start(bf16[512,1024]{1,0:T(8,128)(2,1)} %collective-permute-done.3.refs_4_), channel_id=1, source_target_pairs={{0,4},{1,5},{2,6},{3,7},{4,0},{5,1},{6,2},{7,3},{8,12},{9,13},{10,... | collective-permute-start | bytes 3145736 | tf_op jit(solution)/shard_map/ppermute | solution.py:332
  117.5 29.0 %collective-permute-start.17 = (bf16[512,1024]{1,0:T(8,128)(2,1)}, bf16[512,1024]{1,0:T(8,128)(2,1)}, u32[]{:S(2)}, u32[]{:S(2)}) collective-permute-start(bf16[512,1024]{1,0:T(8,128)(2,1)} %collective-permute-done.16.refs_2_), channel_id=1, source_target_pairs={{0,1},{1,0},{2,3},{3,2},{4,5},{5,4},{6,7},{7,6},{8,9},{9,8},{10,11... | collective-permute-start | bytes 3145736 | tf_op jit(solution)/shard_map/ppermute | solution.py:332
  128.8 19.1 %collective-permute-start.21 = (bf16[512,1024]{1,0:T(8,128)(2,1)}, bf16[512,1024]{1,0:T(8,128)(2,1)}, u32[]{:S(2)}, u32[]{:S(2)}) collective-permute-start(bf16[512,1024]{1,0:T(8,128)(2,1)} %collective-permute-done.20.refs_6_), channel_id=1, source_target_pairs={{0,1},{1,0},{2,3},{3,2},{4,5},{5,4},{6,7},{7,6},{8,9},{9,8},{10,11... | collective-permute-start | bytes 3145736 | tf_op jit(solution)/shard_map/ppermute | solution.py:332
  129.6 14.3 %collective-permute-start.29 = (bf16[2,1024,128]{2,1,0:T(8,128)(2,1)S(1)}, bf16[2,1024,128]{2,1,0:T(8,128)(2,1)S(1)}, u32[]{:S(2)}, u32[]{:S(2)}) collective-permute-start(bf16[2,1024,128]{2,1,0:T(8,128)(2,1)S(1)} %collective-permute-done.28.refs_14_.refs_7_), channel_id=1, source_target_pairs={{0,2},{1,3},{2,0},{3,1},{4,6},{5,7},{6,4},{7,5},{8,10},{9,11},{10,... | collective-permute-start | bytes 1572872 | tf_op jit(solution)/shard_map/ppermute | solution.py:332
  144.8 53.3 %collective-permute-start.4 = (bf16[512,1024]{1,0:T(8,128)(2,1)}, bf16[512,1024]{1,0:T(8,128)(2,1)}, u32[]{:S(2)}, u32[]{:S(2)}) collective-permute-start(bf16[512,1024]{1,0:T(8,128)(2,1)} %collective-permute-done.3.refs_4_), channel_id=1, source_target_pairs={{0,1},{1,0},{2,3},{3,2},{4,5},{5,4},{6,7},{7,6},{8,9},{9,8},{10,11... | collective-permute-start | bytes 3145736 | tf_op jit(solution)/shard_map/ppermute | solution.py:332
  145.8 53.8 %collective-permute-start.2 = (bf16[512,1024]{1,0:T(8,128)(2,1)}, bf16[512,1024]{1,0:T(8,128)(2,1)}, u32[]{:S(2)}, u32[]{:S(2)}) collective-permute-start(bf16[512,1024]{1,0:T(8,128)(2,1)} %collective-permute-done.1.refs_2_), channel_id=1, source_target_pairs={{0,1},{1,0},{2,3},{3,2},{4,5},{5,4},{6,7},{7,6},{8,9},{9,8},{10,11... | collective-permute-start | bytes 3145736 | tf_op jit(solution)/shard_map/ppermute | solution.py:332
  146.5 53.6 %collective-permute-start.6 = (bf16[512,1024]{1,0:T(8,128)(2,1)}, bf16[512,1024]{1,0:T(8,128)(2,1)}, u32[]{:S(2)}, u32[]{:S(2)}) collective-permute-start(bf16[512,1024]{1,0:T(8,128)(2,1)} %collective-permute-done.5.refs_6_), channel_id=1, source_target_pairs={{0,1},{1,0},{2,3},{3,2},{4,5},{5,4},{6,7},{7,6},{8,9},{9,8},{10,11... | collective-permute-start | bytes 3145736 | tf_op jit(solution)/shard_map/ppermute | solution.py:332
  146.5 51.0 %collective-permute-start.13 = (bf16[2,1024,128]{2,1,0:T(8,128)(2,1)}, bf16[2,1024,128]{2,1,0:T(8,128)(2,1)S(1)}, u32[]{:S(2)}, u32[]{:S(2)}) collective-permute-start(bf16[2,1024,128]{2,1,0:T(8,128)(2,1)} %copy-done.35), channel_id=1, source_target_pairs={{0,24},{1,25},{2,26},{3,27},{4,28},{5,29},{6,30},{7,31},{8,16},{9,... | collective-permute-start | bytes 1572872 | tf_op jit(solution)/shard_map/ppermute | solution.py:332
  147.9 48.1 %collective-permute-start.11 = (bf16[2,1024,128]{2,1,0:T(8,128)(2,1)S(1)}, bf16[2,1024,128]{2,1,0:T(8,128)(2,1)S(1)}, u32[]{:S(2)}, u32[]{:S(2)}) collective-permute-start(bf16[2,1024,128]{2,1,0:T(8,128)(2,1)S(1)} %get-tuple-element.77.refs_8_), channel_id=1, source_target_pairs={{0,16},{1,17},{2,18},{3,19},{4,20},{5,21},{6,22},{7,23},{8,24},{9,... | collective-permute-start | bytes 1572872 | tf_op jit(solution)/shard_map/ppermute | solution.py:332
  158.8 38.7 %copy-start.25 = (bf16[2,1024,128]{2,1,0:T(8,128)(2,1)S(1)}, bf16[2,1024,128]{2,1,0:T(8,128)(2,1)}, u32[]{:S(2)}) copy-start(bf16[2,1024,128]{2,1,0:T(8,128)(2,1)} %copy-done.24) | copy-start | bytes 1572868
  158.8 41.3 %copy-start.7 = (bf16[512,1024]{1,0:T(8,128)(2,1)S(1)}, bf16[512,1024]{1,0:T(8,128)(2,1)}, u32[]{:S(2)}) copy-start(bf16[512,1024]{1,0:T(8,128)(2,1)} %copy-done.6) | copy-start | bytes 3145732
  196.0 20.9 %collective-permute-start.8 = (bf16[2,1024,128]{2,1,0:T(8,128)(2,1)S(1)}, bf16[2,1024,128]{2,1,0:T(8,128)(2,1)S(1)}, u32[]{:S(2)}, u32[]{:S(2)}) collective-permute-start(bf16[2,1024,128]{2,1,0:T(8,128)(2,1)S(1)} %get-tuple-element.77.refs_8_), channel_id=1, source_target_pairs={{0,2},{1,3},{2,0},{3,1},{4,6},{5,7},{6,4},{7,5},{8,10},{9,11},{10,... | collective-permute-start | bytes 1572872 | tf_op jit(solution)/shard_map/ppermute | solution.py:332
  197.5 24.5 %collective-permute-start.10 = (bf16[2,1024,128]{2,1,0:T(8,128)(2,1)S(1)}, bf16[2,1024,128]{2,1,0:T(8,128)(2,1)S(1)}, u32[]{:S(2)}, u32[]{:S(2)}) collective-permute-start(bf16[2,1024,128]{2,1,0:T(8,128)(2,1)S(1)} %copy-done.25), channel_id=1, source_target_pairs={{0,2},{1,3},{2,0},{3,1},{4,6},{5,7},{6,4},{7,5},{8,10},{9,11},{10,... | collective-permute-start | bytes 1572872 | tf_op jit(solution)/shard_map/ppermute | solution.py:332
  198.1 35.2 %collective-permute-start.12 = (bf16[2,1024,128]{2,1,0:T(8,128)(2,1)S(1)}, bf16[2,1024,128]{2,1,0:T(8,128)(2,1)S(1)}, u32[]{:S(2)}, u32[]{:S(2)}) collective-permute-start(bf16[2,1024,128]{2,1,0:T(8,128)(2,1)S(1)} %collective-permute-done.11.refs_12_), channel_id=1, source_target_pairs={{0,2},{1,3},{2,0},{3,1},{4,6},{5,7},{6,4},{7,5},{8,10},{9,11},{10,... | collective-permute-start | bytes 1572872 | tf_op jit(solution)/shard_map/ppermute | solution.py:332
  199.6 45.0 %collective-permute-start.14 = (bf16[2,1024,128]{2,1,0:T(8,128)(2,1)S(1)}, bf16[2,1024,128]{2,1,0:T(8,128)(2,1)S(1)}, u32[]{:S(2)}, u32[]{:S(2)}) collective-permute-start(bf16[2,1024,128]{2,1,0:T(8,128)(2,1)S(1)} %collective-permute-done.13.refs_14_), channel_id=1, source_target_pairs={{0,2},{1,3},{2,0},{3,1},{4,6},{5,7},{6,4},{7,5},{8,10},{9,11},{10,... | collective-permute-start | bytes 1572872 | tf_op jit(solution)/shard_map/ppermute | solution.py:332
  215.4 80.0 %collective-permute-start.45 = (bf16[2,1024,128]{2,1,0:T(8,128)(2,1)S(1)}, bf16[2,1024,128]{2,1,0:T(8,128)(2,1)S(1)}, u32[]{:S(2)}, u32[]{:S(2)}) collective-permute-start(bf16[2,1024,128]{2,1,0:T(8,128)(2,1)S(1)} %get-tuple-element.48), channel_id=1, source_target_pairs={{0,2},{1,3},{2,0},{3,1},{4,6},{5,7},{6,4},{7,5},{8,10},{9,11},{10,... | collective-permute-start | bytes 1572872 | tf_op jit(solution)/shard_map/ppermute | solution.py:332
  217.0 116.2 %collective-permute-start.47 = (bf16[2,1024,128]{2,1,0:T(8,128)(2,1)S(1)}, bf16[2,1024,128]{2,1,0:T(8,128)(2,1)S(1)}, u32[]{:S(2)}, u32[]{:S(2)}) collective-permute-start(bf16[2,1024,128]{2,1,0:T(8,128)(2,1)S(1)} %get-tuple-element.50), channel_id=1, source_target_pairs={{0,2},{1,3},{2,0},{3,1},{4,6},{5,7},{6,4},{7,5},{8,10},{9,11},{10,... | collective-permute-start | bytes 1572872 | tf_op jit(solution)/shard_map/ppermute | solution.py:332
  222.1 74.1 %collective-permute-start.48 = (bf16[2,1024,128]{2,1,0:T(8,128)(2,1)S(1)}, bf16[2,1024,128]{2,1,0:T(8,128)(2,1)S(1)}, u32[]{:S(2)}, u32[]{:S(2)}) collective-permute-start(bf16[2,1024,128]{2,1,0:T(8,128)(2,1)S(1)} %get-tuple-element.52), channel_id=1, source_target_pairs={{0,2},{1,3},{2,0},{3,1},{4,6},{5,7},{6,4},{7,5},{8,10},{9,11},{10,... | collective-permute-start | bytes 1572872 | tf_op jit(solution)/shard_map/ppermute | solution.py:332
  233.3 64.6 %collective-permute-start.50 = (bf16[2,1024,128]{2,1,0:T(8,128)(2,1)S(1)}, bf16[2,1024,128]{2,1,0:T(8,128)(2,1)S(1)}, u32[]{:S(2)}, u32[]{:S(2)}) collective-permute-start(bf16[2,1024,128]{2,1,0:T(8,128)(2,1)S(1)} %get-tuple-element.54), channel_id=1, source_target_pairs={{0,2},{1,3},{2,0},{3,1},{4,6},{5,7},{6,4},{7,5},{8,10},{9,11},{10,... | collective-permute-start | bytes 1572872 | tf_op jit(solution)/shard_map/ppermute | solution.py:332
  263.4 17.0 %copy-start.23 = (bf16[2,1024,128]{2,1,0:T(8,128)(2,1)S(1)}, bf16[2,1024,128]{2,1,0:T(8,128)(2,1)}, u32[]{:S(2)}) copy-start(bf16[2,1024,128]{2,1,0:T(8,128)(2,1)} %copy-done.21) | copy-start | bytes 1572868
  263.4 17.0 %copy-start.28 = (bf16[2,1024,128]{2,1,0:T(8,128)(2,1)S(1)}, bf16[2,1024,128]{2,1,0:T(8,128)(2,1)}, u32[]{:S(2)}) copy-start(bf16[2,1024,128]{2,1,0:T(8,128)(2,1)} %copy-done.26) | copy-start | bytes 1572868
  278.8 21.9 %collective-permute-start.37 = (bf16[2,1024,128]{2,1,0:T(8,128)(2,1)S(1)}, bf16[2,1024,128]{2,1,0:T(8,128)(2,1)S(1)}, u32[]{:S(2)}, u32[]{:S(2)}) collective-permute-start(bf16[2,1024,128]{2,1,0:T(8,128)(2,1)S(1)} %get-tuple-element.39), channel_id=1, source_target_pairs={{0,2},{1,3},{2,0},{3,1},{4,6},{5,7},{6,4},{7,5},{8,10},{9,11},{10,... | collective-permute-start | bytes 1572872 | tf_op jit(solution)/shard_map/ppermute | solution.py:332
  295.4 72.4 %collective-permute-start.39 = (bf16[2,1024,128]{2,1,0:T(8,128)(2,1)S(1)}, bf16[2,1024,128]{2,1,0:T(8,128)(2,1)S(1)}, u32[]{:S(2)}, u32[]{:S(2)}) collective-permute-start(bf16[2,1024,128]{2,1,0:T(8,128)(2,1)S(1)} %get-tuple-element.41), channel_id=1, source_target_pairs={{0,2},{1,3},{2,0},{3,1},{4,6},{5,7},{6,4},{7,5},{8,10},{9,11},{10,... | collective-permute-start | bytes 1572872 | tf_op jit(solution)/shard_map/ppermute | solution.py:332
  296.2 27.0 %collective-permute-start.40 = (bf16[2,1024,128]{2,1,0:T(8,128)(2,1)S(1)}, bf16[2,1024,128]{2,1,0:T(8,128)(2,1)S(1)}, u32[]{:S(2)}, u32[]{:S(2)}) collective-permute-start(bf16[2,1024,128]{2,1,0:T(8,128)(2,1)S(1)} %get-tuple-element.43), channel_id=1, source_target_pairs={{0,2},{1,3},{2,0},{3,1},{4,6},{5,7},{6,4},{7,5},{8,10},{9,11},{10,... | collective-permute-start | bytes 1572872 | tf_op jit(solution)/shard_map/ppermute | solution.py:332
  297.9 35.1 %collective-permute-start.42 = (bf16[2,1024,128]{2,1,0:T(8,128)(2,1)S(1)}, bf16[2,1024,128]{2,1,0:T(8,128)(2,1)S(1)}, u32[]{:S(2)}, u32[]{:S(2)}) collective-permute-start(bf16[2,1024,128]{2,1,0:T(8,128)(2,1)S(1)} %get-tuple-element.45), channel_id=1, source_target_pairs={{0,2},{1,3},{2,0},{3,1},{4,6},{5,7},{6,4},{7,5},{8,10},{9,11},{10,... | collective-permute-start | bytes 1572872 | tf_op jit(solution)/shard_map/ppermute | solution.py:332
  300.7 103.0 %collective-permute-start.34 = (bf16[512,1024]{1,0:T(8,128)(2,1)S(1)}, bf16[512,1024]{1,0:T(8,128)(2,1)S(1)}, u32[]{:S(2)}, u32[]{:S(2)}) collective-permute-start(bf16[512,1024]{1,0:T(8,128)(2,1)S(1)} %get-tuple-element.37), channel_id=1, source_target_pairs={{0,1},{1,0},{2,3},{3,2},{4,5},{5,4},{6,7},{7,6},{8,9},{9,8},{10,11... | collective-permute-start | bytes 3145736 | tf_op jit(solution)/shard_map/ppermute | solution.py:332
  323.2 44.5 %collective-permute-start.46 = (bf16[2,1024,128]{2,1,0:T(8,128)(2,1)S(1)}, bf16[2,1024,128]{2,1,0:T(8,128)(2,1)S(1)}, u32[]{:S(2)}, u32[]{:S(2)}) collective-permute-start(bf16[2,1024,128]{2,1,0:T(8,128)(2,1)S(1)} %add_convert_fusion.6), channel_id=1, source_target_pairs={{0,16},{1,17},{2,18},{3,19},{4,20},{5,21},{6,22},{7,23},{8,24},{9,... | collective-permute-start | bytes 1572872 | tf_op jit(solution)/shard_map/ppermute | solution.py:332
  333.0 45.9 %collective-permute-start.38 = (bf16[2,1024,128]{2,1,0:T(8,128)(2,1)S(1)}, bf16[2,1024,128]{2,1,0:T(8,128)(2,1)S(1)}, u32[]{:S(2)}, u32[]{:S(2)}) collective-permute-start(bf16[2,1024,128]{2,1,0:T(8,128)(2,1)S(1)} %add_convert_fusion.9), channel_id=1, source_target_pairs={{0,16},{1,17},{2,18},{3,19},{4,20},{5,21},{6,22},{7,23},{8,24},{9,... | collective-permute-start | bytes 1572872 | tf_op jit(solution)/shard_map/ppermute | solution.py:332
  333.2 45.9 %collective-permute-start.41 = (bf16[2,1024,128]{2,1,0:T(8,128)(2,1)S(1)}, bf16[2,1024,128]{2,1,0:T(8,128)(2,1)S(1)}, u32[]{:S(2)}, u32[]{:S(2)}) collective-permute-start(bf16[2,1024,128]{2,1,0:T(8,128)(2,1)S(1)} %add_convert_fusion.8), channel_id=1, source_target_pairs={{0,24},{1,25},{2,26},{3,27},{4,28},{5,29},{6,30},{7,31},{8,16},{9,... | collective-permute-start | bytes 1572872 | tf_op jit(solution)/shard_map/ppermute | solution.py:332
  367.6 33.6 %collective-permute-start.43 = (bf16[2,1024,128]{2,1,0:T(8,128)(2,1)S(1)}, bf16[2,1024,128]{2,1,0:T(8,128)(2,1)S(1)}, u32[]{:S(2)}, u32[]{:S(2)}) collective-permute-start(bf16[2,1024,128]{2,1,0:T(8,128)(2,1)S(1)} %add_convert_fusion.7), channel_id=1, source_target_pairs={{0,8},{1,9},{2,10},{3,11},{4,12},{5,13},{6,14},{7,15},{8,0},{9,1},... | collective-permute-start | bytes 1572872 | tf_op jit(solution)/shard_map/ppermute | solution.py:332
  367.8 50.1 %collective-permute-start.31 = (bf16[512,1024]{1,0:T(8,128)(2,1)S(1)}, bf16[512,1024]{1,0:T(8,128)(2,1)S(1)}, u32[]{:S(2)}, u32[]{:S(2)}) collective-permute-start(bf16[512,1024]{1,0:T(8,128)(2,1)S(1)} %get-tuple-element.33), channel_id=1, source_target_pairs={{0,1},{1,0},{2,3},{3,2},{4,5},{5,4},{6,7},{7,6},{8,9},{9,8},{10,11... | collective-permute-start | bytes 3145736 | tf_op jit(solution)/shard_map/ppermute | solution.py:332
  378.9 64.2 %collective-permute-start.33 = (bf16[512,1024]{1,0:T(8,128)(2,1)S(1)}, bf16[512,1024]{1,0:T(8,128)(2,1)S(1)}, u32[]{:S(2)}, u32[]{:S(2)}) collective-permute-start(bf16[512,1024]{1,0:T(8,128)(2,1)S(1)} %get-tuple-element.35), channel_id=1, source_target_pairs={{0,1},{1,0},{2,3},{3,2},{4,5},{5,4},{6,7},{7,6},{8,9},{9,8},{10,11... | collective-permute-start | bytes 3145736 | tf_op jit(solution)/shard_map/ppermute | solution.py:332
  379.1 26.6 %collective-permute-start.49 = (bf16[2,1024,128]{2,1,0:T(8,128)(2,1)S(1)}, bf16[2,1024,128]{2,1,0:T(8,128)(2,1)S(1)}, u32[]{:S(2)}, u32[]{:S(2)}) collective-permute-start(bf16[2,1024,128]{2,1,0:T(8,128)(2,1)S(1)} %add_convert_fusion.5), channel_id=1, source_target_pairs={{0,24},{1,25},{2,26},{3,27},{4,28},{5,29},{6,30},{7,31},{8,16},{9,... | collective-permute-start | bytes 1572872 | tf_op jit(solution)/shard_map/ppermute | solution.py:332
  401.2 14.1 %collective-permute-start.51 = (bf16[2,1024,128]{2,1,0:T(8,128)(2,1)S(1)}, bf16[2,1024,128]{2,1,0:T(8,128)(2,1)S(1)}, u32[]{:S(2)}, u32[]{:S(2)}) collective-permute-start(bf16[2,1024,128]{2,1,0:T(8,128)(2,1)S(1)} %add_convert_fusion.4), channel_id=1, source_target_pairs={{0,8},{1,9},{2,10},{3,11},{4,12},{5,13},{6,14},{7,15},{8,0},{9,1},... | collective-permute-start | bytes 1572872 | tf_op jit(solution)/shard_map/ppermute | solution.py:332
  404.1 39.0 %collective-permute-start.35 = (bf16[512,1024]{1,0:T(8,128)(2,1)S(1)}, bf16[512,1024]{1,0:T(8,128)(2,1)S(1)}, u32[]{:S(2)}, u32[]{:S(2)}) collective-permute-start(bf16[512,1024]{1,0:T(8,128)(2,1)S(1)} %add_convert_fusion.2), channel_id=1, source_target_pairs={{0,4},{1,5},{2,6},{3,7},{4,0},{5,1},{6,2},{7,3},{8,12},{9,13},{10,... | collective-permute-start | bytes 3145736 | tf_op jit(solution)/shard_map/ppermute | solution.py:332
  405.7 49.8 %collective-permute-start.30 = (bf16[512,1024]{1,0:T(8,128)(2,1)S(1)}, bf16[512,1024]{1,0:T(8,128)(2,1)}, u32[]{:S(2)}, u32[]{:S(2)}) collective-permute-start(bf16[512,1024]{1,0:T(8,128)(2,1)S(1)} %get-tuple-element.31), channel_id=1, source_target_pairs={{0,1},{1,0},{2,3},{3,2},{4,5},{5,4},{6,7},{7,6},{8,9},{9,8},{10,11... | collective-permute-start | bytes 3145736 | tf_op jit(solution)/shard_map/ppermute | solution.py:332
  415.3 26.1 %collective-permute-start.44 = (bf16[2,1024,128]{2,1,0:T(8,128)(2,1)S(1)}, bf16[2,1024,128]{2,1,0:T(8,128)(2,1)S(1)}, u32[]{:S(2)}, u32[]{:S(2)}) collective-permute-start(bf16[2,1024,128]{2,1,0:T(8,128)(2,1)S(1)} %pad_maximum_fusion.1), channel_id=1, source_target_pairs={{0,4},{1,5},{2,6},{3,7},{4,0},{5,1},{6,2},{7,3},{8,12},{9,13},{10,... | collective-permute-start | bytes 1572872 | tf_op jit(solution)/shard_map/ppermute | solution.py:332
  418.1 34.6 %collective-permute-start.52 = (bf16[2,1024,128]{2,1,0:T(8,128)(2,1)}, bf16[2,1024,128]{2,1,0:T(8,128)(2,1)}, u32[]{:S(2)}, u32[]{:S(2)}) collective-permute-start(bf16[2,1024,128]{2,1,0:T(8,128)(2,1)} %pad_maximum_fusion.2), channel_id=1, source_target_pairs={{0,4},{1,5},{2,6},{3,7},{4,0},{5,1},{6,2},{7,3},{8,12},{9,13},{10,... | collective-permute-start | bytes 1572872 | tf_op jit(solution)/shard_map/ppermute | solution.py:332
  441.4 32.3 %collective-permute-start.32 = (bf16[512,1024]{1,0:T(8,128)(2,1)}, bf16[512,1024]{1,0:T(8,128)(2,1)}, u32[]{:S(2)}, u32[]{:S(2)}) collective-permute-start(bf16[512,1024]{1,0:T(8,128)(2,1)} %add_convert_fusion.3), channel_id=1, source_target_pairs={{0,4},{1,5},{2,6},{3,7},{4,0},{5,1},{6,2},{7,3},{8,12},{9,13},{10,... | collective-permute-start | bytes 3145736 | tf_op jit(solution)/shard_map/ppermute | solution.py:332
  444.7 29.0 %collective-permute-start.36 = (bf16[512,1024]{1,0:T(8,128)(2,1)}, bf16[512,1024]{1,0:T(8,128)(2,1)}, u32[]{:S(2)}, u32[]{:S(2)}) collective-permute-start(bf16[512,1024]{1,0:T(8,128)(2,1)} %add_convert_fusion.1), channel_id=1, source_target_pairs={{0,8},{1,9},{2,10},{3,11},{4,12},{5,13},{6,14},{7,15},{8,0},{9,1},... | collective-permute-start | bytes 3145736 | tf_op jit(solution)/shard_map/ppermute | solution.py:332
  (25 other events, 112.8 us)
